TPU v7x, 32 devices: a whole 2x2x4 slice. The times are simulated.
32 devices in a mesh: ep: 16 (over z, y, x), tp: 2 (over core).
Axes of the slice: x: 2, y: 2, z: 4, core: 2. Of those that a mesh axis runs over, the one named last changes fastest.
Arguments:
- stream: bfloat16 [512, 2048], P('ep'), may hold values from -6 to 6
- mixer_gain: float32 [2048], replicated, may hold values from 0.1 to 1.9
- gate_proj: bfloat16 [2048, 1024], P(None, 'tp'), may hold values from -0.125 to 0.125
- input_proj: bfloat16 [2048, 1024], P(None, 'tp'), may hold values from -0.125 to 0.125
- state_maps: bfloat16 [2, 2048, 256], P(None, None, 'tp'), may hold values from -0.125 to 0.125
- step_proj: bfloat16 [2048, 16], P(None, 'tp'), may hold values from -0.125 to 0.125
- step_bias: float32 [16], P('tp'), may hold values from -3 to 0.5
- decay_rate: float32 [16], P('tp'), may hold values from 0.05 to 4
- input_taps: float32 [4, 1024], P(None, 'tp'), may hold values from -3 to 3
- map_taps: float32 [2, 4, 256], P(None, None, 'tp'), may hold values from -3 to 3
- input_past: bfloat16 [512, 3, 1024], P('ep', None, 'tp'), may hold values from -6 to 6
- map_past: bfloat16 [512, 2, 3, 256], P('ep', None, None, 'tp'), may hold values from -6 to 6
- head_state: float32 [512, 16, 4096], P('ep', 'tp'), may hold values from -1.6 to 1.6
- skip_gain: float32 [16], P('tp'), may hold values from 0 to 2
- inner_gain: float32 [1024], P('tp'), may hold values from 0.1 to 1.9
- mixer_out: bfloat16 [1024, 2048], P('tp'), may hold values from -0.1875 to 0.1875
- channel_gain: float32 [2048], replicated, may hold values from 0.1 to 1.9
- expert_ids: int32 [512, 2], P('ep'), may hold values from 0 to 7, all different within a row; in each aligned block of 32 rows (0 to 31, 32 to 63, ...) at most 12 rows name the same one
- expert_weight: float32 [512, 2], P('ep'), may hold values from 0.2 to 1
- expert_gate: bfloat16 [2048, 57344], P(None, ('ep', 'tp')), may hold values from -0.125 to 0.125
- expert_up: bfloat16 [2048, 57344], P(None, ('ep', 'tp')), may hold values from -0.125 to 0.125
- expert_down: bfloat16 [57344, 2048], P(('ep', 'tp')), may hold values from -0.0625 to 0.0625
- dense_gate: bfloat16 [2048, 5632], P('tp', 'ep'), may hold values from -0.125 to 0.125
- dense_up: bfloat16 [2048, 5632], P('tp', 'ep'), may hold values from -0.125 to 0.125
- dense_down: bfloat16 [5632, 2048], P('ep', 'tp'), may hold values from -0.078125 to 0.078125
- dense_mix: float32 [2048], P('tp'), may hold values from -2 to 2
Outputs:
- stream_out: bfloat16 [512, 2048], P('ep', 'tp')
- state_out: float32 [512, 16, 4096], P('ep', 'tp')
Inputs may be any that keep to these rules, and one draw needn't show every extreme that they name: `expert_ids`: each row names 2 different experts. In each aligned block of 32 rows no expert is named by more than 12 rows, and in some block one expert is named by exactly 12 rows.
All inputs are finite; a program needn't handle non-finite values.
Results may differ from a plain program's by a relative error of at most 0.015.
Values may be sent and summed in bfloat16 or wider, within the bound.
A program may use at most 128 MiB of HBM per device.

v0:
```python
import functools

import jax
import jax.numpy as jnp
from jax import lax
from jax.experimental import pallas as pl
from jax.experimental.pallas import tpu as pltpu
from jax.sharding import PartitionSpec as P

HEAD = 64
HEADS = 16
GROUPS = 4
NSTATE = 64
EXPERTS = 8
TOP_K = 2
CAP = 12


EPS = 1e-06


def rms_scale(values):
    return values * lax.rsqrt(jnp.mean(values * values, axis=-1, keepdims=True) + EPS)


def short_conv(past_rows, newest, tap_weights, along):
    window = jnp.concatenate([past_rows, jnp.expand_dims(newest, along)], axis=along).astype(
        jnp.float32
    )
    return jax.nn.silu(jnp.sum(window * tap_weights, axis=along))


def three_parts(value):
    high = value.astype(jnp.bfloat16)
    rest = value - high.astype(jnp.float32)
    middle = rest.astype(jnp.bfloat16)
    return high, middle, (rest - middle.astype(jnp.float32)).astype(jnp.bfloat16)


def state_kernel(state, fed, write, read_by, decay, state_out, read, picks):
    lanes = state.shape[1]

    @pl.when(pl.program_id(0) == 0)
    def _():
        rows_of = lax.broadcasted_iota(jnp.int32, picks.shape, 0)
        owner = lax.broadcasted_iota(jnp.int32, picks.shape, 1) // NSTATE
        picks[...] = jnp.where(rows_of == owner, 1.0, 0.0).astype(jnp.bfloat16)

    width = 4 * 128
    copies = width // NSTATE
    fed_parts = three_parts(fed[...])
    write_wide = jnp.concatenate([write[...]] * copies, axis=1)
    read_wide = jnp.concatenate([read_by[...]] * copies, axis=1)
    decay_wide = jnp.concatenate([decay[...]] * (width // 128), axis=1)
    total = jnp.zeros(read.shape, jnp.float32)
    for at in range(0, lanes, width):
        cut = slice(at, at + width)
        pick = picks[:, cut]
        fed_wide = sum(
            jnp.dot(part, pick, preferred_element_type=jnp.float32) for part in fed_parts[::-1]
        )
        value = decay_wide * state[:, cut] + fed_wide * write_wide
        state_out[:, cut] = value
        for part in three_parts(value * read_wide):
            total = total + lax.dot_general(
                part, pick, (((1,), (1,)), ((), ())), preferred_element_type=jnp.float32
            )
    read[...] = total


def step_state(state, fed, write, read_by, decay):
    flat, lanes = state.shape
    rows = 64

    def block(array):
        return pl.BlockSpec((rows, array.shape[1]), lambda i: (i, 0))

    return pl.pallas_call(
        state_kernel,
        grid=(flat // rows,),
        out_shape=(
            jax.ShapeDtypeStruct(state.shape, jnp.float32),
            jax.ShapeDtypeStruct(fed.shape, jnp.float32),
        ),
        in_specs=[block(x) for x in (state, fed, write, read_by, decay)],
        out_specs=(block(state), block(fed)),
        scratch_shapes=[pltpu.VMEM((HEAD, lanes), jnp.bfloat16)],
        compiler_params=pltpu.CompilerParams(
            dimension_semantics=("arbitrary",), vmem_limit_bytes=16 * 1024 * 1024
        ),
        name="state",
    )(state, fed, write, read_by, decay)


def mix_heads(
    stream,
    mixer_gain,
    gate_proj,
    input_proj,
    state_maps,
    step_proj,
    step_bias,
    decay_rate,
    input_taps,
    map_taps,
    input_past,
    map_past,
    head_state,
    skip_gain,
    inner_gain,
):
    row_count = stream.shape[0]
    normed = (rms_scale(stream.astype(jnp.float32)) * mixer_gain).astype(jnp.bfloat16)
    gate_in = jnp.dot(normed, gate_proj, preferred_element_type=jnp.float32).astype(jnp.bfloat16)
    input_new = jnp.dot(normed, input_proj, preferred_element_type=jnp.float32).astype(jnp.bfloat16)
    map_new = jnp.stack(
        [
            jnp.dot(normed, state_maps[0], preferred_element_type=jnp.float32),
            jnp.dot(normed, state_maps[1], preferred_element_type=jnp.float32),
        ],
        axis=1,
    ).astype(jnp.bfloat16)
    step_size = jax.nn.softplus(
        jnp.dot(normed, step_proj, preferred_element_type=jnp.float32) + step_bias
    )
    conv_in = short_conv(input_past, input_new, input_taps, 1)
    conv_map = short_conv(map_past, map_new, map_taps, 2)
    head_count = step_size.shape[1]
    per_group = HEADS // GROUPS
    group_count = head_count // per_group
    values = conv_in.reshape(row_count, head_count, HEAD)
    decay_now = jnp.exp(-decay_rate * step_size)
    flat = row_count * head_count

    def by_head(maps):
        maps = maps.reshape(row_count, group_count, 1, NSTATE)
        return jnp.broadcast_to(
            maps, (row_count, group_count, per_group, NSTATE)
        ).reshape(flat, NSTATE)

    state_new, read = step_state(
        head_state.reshape(flat, HEAD * NSTATE),
        (step_size[:, :, None] * values).reshape(flat, HEAD),
        by_head(conv_map[:, 0]),
        by_head(conv_map[:, 1]),
        jnp.broadcast_to(decay_now[:, :, None], (row_count, head_count, 128)).reshape(flat, 128),
    )
    gated = read.reshape(row_count, head_count, HEAD) + skip_gain[:, None] * values
    gated = gated.reshape(row_count, head_count * HEAD) * jax.nn.silu(gate_in.astype(jnp.float32))
    inner_out = (
        rms_scale(gated.reshape(row_count, group_count, -1)).reshape(row_count, -1) * inner_gain
    )
    return (
        inner_out.astype(jnp.bfloat16),
        state_new.reshape(row_count, head_count, HEAD * NSTATE),
    )


MESH = pl.DeviceIdType.MESH


def grid_of(ep_count):
    side = 4 if ep_count % 64 == 0 else (2 if ep_count % 4 == 0 else 1)
    return side, ep_count // (side * side)


class Place:
    def __init__(self, ep_count):
        self.side, self.line = grid_of(ep_count)
        self.ep = lax.axis_index("ep")
        self.core = lax.axis_index("tp")
        col = self.ep % self.side
        row = (self.ep // self.side) % self.side
        self.z = self.ep // (self.side * self.side)
        self.a = row * (1 - self.core) + col * self.core
        self.b = col * (1 - self.core) + row * self.core
        self.row, self.col = row, col

    def at(self, db, da, dz, core=None):
        core = self.core if core is None else core
        a = self.row * (1 - core) + self.col * core
        b = self.col * (1 - core) + self.row * core
        a = (a + da) % self.side
        b = (b + db) % self.side
        z = (self.z + dz) % self.line
        row = a * (1 - core) + b * core
        col = b * (1 - core) + a * core
        return (z * self.side + row) * self.side + col

    def near(self, db, da, dz):
        return {"ep": self.at(db, da, dz), "tp": self.core}

    def sibling(self):
        return {"ep": self.ep, "tp": 1 - self.core}

    def z_order(self):
        line = self.line
        return sorted(range(1, line), key=lambda d: (min(d, line - d), d))

    def partners(self):
        side = range(1, self.side)
        return (
            [self.near(d, 0, 0) for d in side]
            + [self.near(0, d, 0) for d in side]
            + [self.near(0, 0, d) for d in self.z_order()]
        )


def greet(targets):
    barrier = pltpu.get_barrier_semaphore()
    for target in targets:
        pl.semaphore_signal(barrier, inc=1, device_id=target, device_id_type=MESH)
    pl.semaphore_wait(barrier, len(targets))


def spread_kernel(ep_count, partial, stream, gain, meta, every, notes, kept, other, *sems):
    part_send, part_recv, note_send, note_recv, link_send, link_recv, core_send, core_recv = sems
    place = Place(ep_count)
    side, line = place.side, place.line
    half = every.shape[3]
    me = place.ep
    everyone = [{"ep": (me + d) % ep_count, "tp": place.core} for d in range(1, ep_count)]
    greet([place.sibling()] + everyone)
    sends = []

    def send(src, dst, send_sem, recv_sem, target):
        copy = pltpu.make_async_remote_copy(
            src_ref=src, dst_ref=dst, send_sem=send_sem, recv_sem=recv_sem,
            device_id=target, device_id_type=MESH,
        )
        copy.start()
        sends.append(copy)
        return copy

    swap = send(partial, other, part_send, part_recv, place.sibling())
    for d in range(1, ep_count):
        send(meta, notes.at[me], note_send.at[d - 1], note_recv.at[d - 1], everyone[d - 1])
    notes[me] = meta[...]
    swap.wait_recv()
    hidden = stream[...].astype(jnp.float32) + (
        partial[...].astype(jnp.float32) + other[...].astype(jnp.float32)
    )
    ffn_in = (rms_scale(hidden) * gain[...]).astype(jnp.bfloat16)
    first = place.core == 0
    kept[...] = jnp.where(first, hidden[:, :half], hidden[:, half:])
    every[0, me] = jnp.where(first, ffn_in[:, :half], ffn_in[:, half:])
    every[1, me] = jnp.where(first, ffn_in[:, half:], ffn_in[:, :half])

    def slot(db, da, dz):
        return ((db % side) * side + da % side) * line + dz % line

    used = [0]

    def pass_on(off, step):
        block = every.at[0, place.at(*off)]
        there = slot(*(o - s for o, s in zip(off, step)))
        send(block, block, link_send.at[used[0]], link_recv.at[there], place.near(*step))
        used[0] += 1

    def arrived(off):
        block = every.at[0, place.at(*off)]
        at = slot(*off)
        pltpu.make_async_copy(block, block, link_recv.at[at]).wait()
        send(block, every.at[1, place.at(*off)], core_send.at[at], core_recv.at[at], place.sibling())

    for dz in place.z_order():
        pass_on((0, 0, 0), (0, 0, dz))
    zs = [0] + place.z_order()
    for dz in zs:
        if dz:
            arrived((0, 0, dz))
        for d in range(1, side):
            pass_on((0, 0, dz), (0, d, 0))
        for d in range(1, side):
            pass_on((0, 0, dz), (d, 0, 0))
    for dz in zs:
        for da in range(1, side):
            arrived((0, da, dz))
            for d in range(1, side):
                pass_on((0, da, dz), (d, 0, 0))
    for dz in zs:
        for da in range(side):
            for db in range(1, side):
                arrived((db, da, dz))
    for d in range(1, ep_count):
        source = (me + ep_count - d) % ep_count
        pltpu.make_async_copy(notes.at[source], notes.at[source], note_recv.at[d - 1]).wait()
    for at in range(1, ep_count):
        dz, rest = at % line, at // line
        source = place.at(rest // side, rest % side, dz, 1 - place.core)
        block = every.at[1, source]
        pltpu.make_async_copy(block, block, core_recv.at[at]).wait()
    for copy in sends:
        copy.wait_send()


def spread(partial, stream, gain, meta):
    ep_count = lax.axis_size("ep")
    rows, width = stream.shape
    half = width // 2
    vmem = pl.BlockSpec(memory_space=pltpu.VMEM)
    dma = pltpu.SemaphoreType.DMA
    return pl.pallas_call(
        functools.partial(spread_kernel, ep_count),
        out_shape=(
            jax.ShapeDtypeStruct((2, ep_count, rows, half), jnp.bfloat16),
            jax.ShapeDtypeStruct((ep_count,) + meta.shape, jnp.float32),
            jax.ShapeDtypeStruct((rows, half), jnp.float32),
        ),
        in_specs=[vmem] * 4,
        out_specs=(vmem,) * 3,
        scratch_shapes=[
            pltpu.VMEM((rows, width), jnp.bfloat16),
            dma, dma,
            dma((ep_count,)), dma((ep_count,)),
            dma((ep_count,)), dma((ep_count,)),
            dma((ep_count,)), dma((ep_count,)),
        ],
        compiler_params=pltpu.CompilerParams(
            collective_id=1, has_side_effects=True, vmem_limit_bytes=grant(ep_count)
        ),
        name="spread",
    )(partial, stream, gain, meta)


def collect_kernel(ep_count, own, theirs, kept, out, held, total, from_b, from_a, from_z, *sems):
    core_send, core_recv, link_send, recv_b, recv_a, recv_z = sems
    place = Place(ep_count)
    side, line = place.side, place.line
    greet([place.sibling()] + place.partners())
    zs = place.z_order() + [0]
    spots = [(db, da, dz) for dz in zs for da in range(side) for db in range(1, side)]
    spots += [(0, da, dz) for dz in zs for da in range(1, side)]
    spots += [(0, 0, dz) for dz in zs]
    sends = []

    def send(src, dst, send_sem, recv_sem, target):
        copy = pltpu.make_async_remote_copy(
            src_ref=src, dst_ref=dst, send_sem=send_sem, recv_sem=recv_sem,
            device_id=target, device_id_type=MESH,
        )
        copy.start()
        sends.append(copy)

    for at, off in enumerate(spots):
        send(
            theirs.at[place.at(*off, 1 - place.core)], held.at[at],
            core_send.at[at], core_recv.at[at], place.sibling(),
        )

    def take(ref, sem):
        pltpu.make_async_copy(ref, ref, sem).wait()
        return ref[...].astype(jnp.float32)

    for at, (db, da, dz) in enumerate(spots):
        value = own[place.at(db, da, dz)].astype(jnp.float32)
        value = value + take(held.at[at], core_recv.at[at])
        if db:
            total[at] = value.astype(jnp.bfloat16)
            send(
                total.at[at], from_b.at[db - 1, da, dz],
                link_send.at[at], recv_b.at[db - 1, da, dz], place.near(db, 0, 0),
            )
            continue
        for d in range(1, side):
            value = value + take(from_b.at[d - 1, da, dz], recv_b.at[d - 1, da, dz])
        if da:
            total[at] = value.astype(jnp.bfloat16)
            send(
                total.at[at], from_a.at[da - 1, dz],
                link_send.at[at], recv_a.at[da - 1, dz], place.near(0, da, 0),
            )
            continue
        for d in range(1, side):
            value = value + take(from_a.at[d - 1, dz], recv_a.at[d - 1, dz])
        if dz:
            total[at] = value.astype(jnp.bfloat16)
            send(
                total.at[at], from_z.at[dz - 1],
                link_send.at[at], recv_z.at[dz - 1], place.near(0, 0, dz),
            )
            continue
        for d in range(1, line):
            value = value + take(from_z.at[d - 1], recv_z.at[d - 1])
        out[...] = (kept[...] + value).astype(out.dtype)
    for copy in sends:
        copy.wait_send()


def collect(own, theirs, kept):
    ep_count = lax.axis_size("ep")
    side, line = grid_of(ep_count)
    rows, half = kept.shape
    vmem = pl.BlockSpec(memory_space=pltpu.VMEM)
    dma = pltpu.SemaphoreType.DMA
    more = max(side - 1, 1)
    block = (rows, half)
    return pl.pallas_call(
        functools.partial(collect_kernel, ep_count),
        out_shape=jax.ShapeDtypeStruct((rows, half), jnp.bfloat16),
        in_specs=[vmem] * 3,
        out_specs=vmem,
        scratch_shapes=[
            pltpu.VMEM((ep_count,) + block, jnp.bfloat16),
            pltpu.VMEM((ep_count,) + block, jnp.bfloat16),
            pltpu.VMEM((more, side, line) + block, jnp.bfloat16),
            pltpu.VMEM((more, line) + block, jnp.bfloat16),
            pltpu.VMEM((max(line - 1, 1),) + block, jnp.bfloat16),
            dma((ep_count,)), dma((ep_count,)), dma((ep_count,)),
            dma((more, side, line)), dma((more, line)), dma((max(line - 1, 1),)),
        ],
        compiler_params=pltpu.CompilerParams(
            collective_id=2, has_side_effects=True, vmem_limit_bytes=grant(ep_count)
        ),
        name="collect",
    )(own.reshape((ep_count,) + block), theirs.reshape((ep_count,) + block), kept)


def grant(ep_count):
    return max(8, ep_count // 2) * 1024 * 1024


def local(
    stream,
    mixer_gain,
    gate_proj,
    input_proj,
    state_maps,
    step_proj,
    step_bias,
    decay_rate,
    input_taps,
    map_taps,
    input_past,
    map_past,
    head_state,
    skip_gain,
    inner_gain,
    mixer_out,
    channel_gain,
    expert_ids,
    expert_weight,
    expert_gate,
    expert_up,
    expert_down,
    dense_gate,
    dense_up,
    dense_down,
    dense_mix,
):
    core = lax.axis_index("tp")
    first = core == 0
    swap = [(0, 1), (1, 0)]
    units = dense_gate.shape[1] // 2

    def mine(left, right):
        return jnp.where(first, left, right)

    low = jnp.concatenate([dense_gate[:, :units], dense_up[:, :units]], axis=1)
    high = jnp.concatenate([dense_gate[:, units:], dense_up[:, units:]], axis=1)
    wide_own = mine(low, high)
    wide_other = lax.ppermute(mine(high, low), "tp", swap)
    down_own = mine(dense_down[:units], dense_down[units:])
    down_other = lax.ppermute(mine(dense_down[units:], dense_down[:units]), "tp", swap)
    mix_other = lax.ppermute(dense_mix, "tp", swap)

    inner_out, state_out = mix_heads(
        stream, mixer_gain, gate_proj, input_proj, state_maps, step_proj, step_bias, decay_rate,
        input_taps, map_taps, input_past, map_past, head_state, skip_gain, inner_gain,
    )
    partial_out = jnp.dot(inner_out, mixer_out, preferred_element_type=jnp.float32)

    row_count, width = stream.shape
    half = width // 2
    named = expert_ids[:, :, None] == jnp.arange(EXPERTS, dtype=jnp.int32)
    weight = jnp.sum(jnp.where(named, expert_weight[:, :, None], 0.0), axis=1)
    hits = jnp.any(named, axis=1)
    earlier = jnp.tril(jnp.ones((row_count, row_count), jnp.bfloat16), -1)
    rank = jnp.dot(earlier, hits.astype(jnp.bfloat16), preferred_element_type=jnp.float32)
    rank = jnp.where(hits, rank, -1.0)
    lanes = -(-2 * row_count // 128) * 128
    meta = jnp.concatenate([rank.T, weight.T], axis=1)
    meta = jnp.pad(meta, ((0, 0), (0, lanes - 2 * row_count)))

    every, notes, kept = spread(
        partial_out.astype(jnp.bfloat16), stream, channel_gain[None, :], meta
    )

    ep_count = lax.axis_size("ep")
    total_rows = ep_count * row_count
    slots = ep_count * CAP
    expert = lax.axis_index("ep") // (ep_count // EXPERTS)
    notes = lax.dynamic_index_in_dim(notes, expert, 1, keepdims=False)
    rank_all = notes[:, :row_count].reshape(1, total_rows)
    weight_all = notes[:, row_count : 2 * row_count].reshape(1, total_rows)
    slot_ids = jnp.arange(slots, dtype=jnp.int32)[:, None]
    row_ids = jnp.arange(total_rows, dtype=jnp.int32)[None, :]
    match = (slot_ids // CAP == row_ids // row_count) & (
        (slot_ids % CAP).astype(jnp.float32) == rank_all
    )
    slot_weight = jnp.sum(jnp.where(match, weight_all, 0.0), axis=1, keepdims=True)
    pick = match.astype(jnp.bfloat16)
    all_own = every[0].reshape(total_rows, half)
    all_other = every[1].reshape(total_rows, half)

    def f32_dot(left, right):
        return jnp.dot(left, right, preferred_element_type=jnp.float32)

    rows_own = f32_dot(pick, all_own).astype(jnp.bfloat16)
    rows_other = f32_dot(pick, all_other).astype(jnp.bfloat16)
    rows = jnp.concatenate([mine(rows_own, rows_other), mine(rows_other, rows_own)], axis=1)
    act = (jax.nn.silu(f32_dot(rows, expert_gate)) * f32_dot(rows, expert_up)).astype(jnp.bfloat16)
    share = (f32_dot(act, expert_down) * slot_weight).astype(jnp.bfloat16)
    share_own = mine(share[:, :half], share[:, half:])
    share_other = mine(share[:, half:], share[:, :half])

    wide = f32_dot(all_own, wide_own) + f32_dot(all_other, wide_other)
    dense_act = (jax.nn.silu(wide[:, :units]) * wide[:, units:]).astype(jnp.bfloat16)

    def result(share_half, down_half, mix_half):
        spread_back = lax.dot_general(
            pick, share_half, (((0,), (0,)), ((), ())), preferred_element_type=jnp.float32
        )
        dense = f32_dot(dense_act, down_half) * jax.nn.sigmoid(mix_half)
        return (spread_back + dense).astype(jnp.bfloat16)

    updated = collect(
        result(share_own, down_own, dense_mix),
        result(share_other, down_other, mix_other),
        kept,
    )
    return (updated, state_out)


def solution(mesh):
    placed = (
        P("ep", None),
        P(),
        P(None, "tp"),
        P(None, "tp"),
        P(None, None, "tp"),
        P(None, "tp"),
        P("tp"),
        P("tp"),
        P(None, "tp"),
        P(None, None, "tp"),
        P("ep", None, "tp"),
        P("ep", None, None, "tp"),
        P("ep", "tp", None),
        P("tp"),
        P("tp"),
        P("tp", None),
        P(),
        P("ep", None),
        P("ep", None),
        P(None, ("ep", "tp")),
        P(None, ("ep", "tp")),
        P(("ep", "tp"), None),
        P("tp", "ep"),
        P("tp", "ep"),
        P("ep", "tp"),
        P("tp"),
    )
    return jax.shard_map(
        local,
        mesh=mesh,
        in_specs=placed,
        out_specs=(P("ep", "tp"), P("ep", "tp", None)),
        check_vma=False,
    )
```

profile of v0, /device:TPU:0, one launch (start us, length us, event | category | flops | bytes accessed | tf_op | source)
XLA Modules:
  0.0 100.2 jit_solution(3819821595114738175)
XLA Ops:
  0.6 0.6 collective-permute-start.2
  1.2 1.9 %broadcast_select_fusion.3 = bf16[176,1024]{1,0:T(8,128)(2,1)} fusion(pred[]{:T(512)S(6)} %eq.56, bf16[352,1024]{1,0:T(8,128)(2,1)} %param.50), kind=kLoop, calls=%fused_computation.45 | loop fusion | flops 180224 | bytes 1081345 | tf_op jit(solution)/shard_map/jit(_where)/select_n | solution.py:457
  3.2 0.1 collective-permute-start.1
  3.2 1.4 %fusion.58 = (bf16[1024,176]{0,1:T(8,128)(2,1)S(1)}, bf16[1024,176]{0,1:T(8,128)(2,1)S(1)}, bf16[1024,176]{0,1:T(8,128)(2,1)S(1)}, bf16[1024,176]{0,1:T(8,128)(2,1)S(1)}) fusion(bf16[1024,352]{0,1:T(8,128)(2,1)} %param.48, bf16[1024,352]{0,1:T(8,128)(2,1)} %param.49), kind=kLoop, calls=%fused_computation.108 | loop fusion | bytes 2883584 | tf_op jit(solution)/shard_map/slice | solution.py:459
  4.8 0.6 copy-done.6
  5.4 1.1 %broadcast_select_fusion = bf16[1024,352]{0,1:T(8,128)(2,1)} fusion(pred[]{:T(512)S(6)} %eq.56, bf16[1024,176]{0,1:T(8,128)(2,1)S(1)} %get-tuple-element.30, bf16[1024,176]{0,1:T(8,128)(2,1)S(1)} %get-tuple-element.19, bf16[1024,176]{0,1:T(8,128)(2,1)S(1)} %get-tuple-element.31, bf16[1024,176]{0,1:T(8,128)(2,1)S(1)} %get-tuple-element.18), kind=kLoop, calls=%fused_computation.25 | loop fusion | flops 3244032 | bytes 2162689 | tf_op jit(solution)/shard_map/jit(_where)/select_n | solution.py:457
  6.5 0.5 collective-permute-start
  7.0 0.1 fusion.29
  7.2 1.3 %fusion.4 = bf16[32,1,1,128]{3,0,2,1:T(8,128)(2,1)S(1)} fusion(bf16[2,2048,128]{2,1,0:T(8,128)(2,1)} %param.30, bf16[32,2048]{1,0:T(8,128)(2,1)S(1)} %copy-done.2, f32[2048]{0:T(1024)S(1)} %copy-done.18, f32[32]{0:T(128)S(1)} %add_rsqrt_fusion.1), kind=kOutput, calls=%fused_computation.16 | convolution fusion | flops 17043456 | bytes 671872 | tf_op jit(solution)/shard_map/dot_general | solution.py:118
  8.5 1.3 %fusion.5 = bf16[32,1,1,128]{3,0,2,1:T(8,128)(2,1)S(1)} fusion(bf16[2,2048,128]{2,1,0:T(8,128)(2,1)} %param.30, bf16[32,2048]{1,0:T(8,128)(2,1)S(1)} %copy-done.2, f32[2048]{0:T(1024)S(1)} %copy-done.18, f32[32]{0:T(128)S(1)} %add_rsqrt_fusion.1), kind=kOutput, calls=%fused_computation.17 | convolution fusion | flops 17043456 | bytes 671872 | tf_op jit(solution)/shard_map/dot_general | solution.py:119
  10.2 0.1 multiply_reduce_fusion.1
  10.4 0.2 multiply_exponential_fusion
  10.7 0.1 broadcast_in_dim.88
  10.8 0.1 broadcast_in_dim.86
  11.0 0.1 mul.154
  11.1 0.1 broadcast_in_dim.84
  11.2 2.1 %fusion.3 = bf16[32,1,512]{2,0,1:T(8,128)(2,1)S(1)} fusion(bf16[2048,512]{1,0:T(8,128)(2,1)} %param.29, bf16[32,2048]{1,0:T(8,128)(2,1)S(1)} %copy-done.2, f32[2048]{0:T(1024)S(1)} %copy-done.18, f32[32]{0:T(128)S(1)} %add_rsqrt_fusion.1), kind=kOutput, calls=%fused_computation.13 | convolution fusion | flops 67387392 | bytes 2269312 | tf_op jit(solution)/shard_map/dot_general | solution.py:115
  13.4 0.1 multiply_multiply_fusion.fed
  13.6 0.1 broadcast_in_dim.89.decay
  13.7 2.2 %copy-done.1 = f32[32,8,4096]{2,1,0:T(8,128)S(1)} copy-done((f32[32,8,4096]{2,1,0:T(8,128)S(1)}, f32[32,8,4096]{2,1,0:T(8,128)}, u32[]{:S(2)}) %copy-start.1) | copy-done | bytes 4194328
  15.9 5.8 %state.1 = (f32[256,4096]{1,0:T(8,128)}, f32[256,64]{1,0:T(8,128)S(1)}) custom-call(f32[256,4096]{1,0:T(8,128)S(1)} %bitcast.44, f32[256,64]{1,0:T(8,128)S(1)} %multiply_multiply_fusion.fed, f32[256,64]{1,0:T(8,128)S(1)} %bitcast.46, f32[256,64]{1,0:T(8,128)S(1)} %bitcast.47, f32[256,128]{1,0:T(8,128)S(1)} %broadcast_in_dim.89.decay), custom_call_target="tpu_custom_call" | custom-call | tf_op jit(solution)/shard_map/state/pallas_call | solution.py:78
  21.7 0.1 reshape.187
  21.8 2.1 %fusion.61 = (f32[32,512]{1,0:T(8,128)S(1)}, f32[32,512]{1,0:T(8,128)S(1)}) fusion(bf16[2048,512]{1,0:T(8,128)(2,1)} %param.28, bf16[32,2048]{1,0:T(8,128)(2,1)S(1)} %copy-done.2, f32[2048]{0:T(1024)S(1)} %copy-done.18, f32[32]{0:T(128)S(1)} %add_rsqrt_fusion.1, f32[32,512]{1,0:T(8,128)S(1)} %reshape.187, f32[32,512]{1,0:T(8,128)S(1)} %multiply_reduce_fusion, ...), kind=kOutput, calls=%fused_computation.111 | convolution fusion | flops 67600384 | bytes 2500736 | tf_op jit(solution)/shard_map/dot_general | solution.py:114
  24.0 0.1 reduce_sum.60
  24.1 0.1 mul.174
  24.2 0.2 convolution_select_fusion
  24.5 0.5 convolution_convert_fusion.partial
  25.0 23.2 %spread.1 = (bf16[2,16,32,1024]{3,2,1,0:T(8,128)(2,1)S(1)}, f32[16,8,128]{2,1,0:T(8,128)S(1)}, f32[32,1024]{1,0:T(8,128)S(1)}) custom-call(bf16[32,2048]{1,0:T(8,128)(2,1)S(1)} %convolution_convert_fusion.partial, bf16[32,2048]{1,0:T(8,128)(2,1)S(1)} %copy-done.2, f32[1,2048]{1,0:T(1,128)S(1)} %bitcast.48, f32[8,128]{1,0:T(8,128)S(1)} %select_maximum_fusion.meta), custom_call_target="tpu_custom_call" | custom-call | tf_op jit(solution)/shard_map/spread/pallas_call | solution.py:303
  48.2 1.3 %copy-done.3 = bf16[2,16,32,1024]{3,2,1,0:T(8,128)(2,1)} copy-done((bf16[2,16,32,1024]{3,2,1,0:T(8,128)(2,1)}, bf16[2,16,32,1024]{3,2,1,0:T(8,128)(2,1)S(1)}, u32[]{:S(2)}) %copy-start.3) | copy-done | bytes 2097176
  49.8 1.7 %fusion.57 = (bf16[1,16,32,1024]{3,2,1,0:T(8,128)(2,1)S(1)}, bf16[1,16,32,1024]{3,2,1,0:T(8,128)(2,1)S(1)}) fusion(bf16[2,16,32,1024]{3,2,1,0:T(8,128)(2,1)} %copy-done.3), kind=kLoop, calls=%fused_computation.107 | loop fusion | bytes 4194304 | tf_op jit(solution)/shard_map/slice | solution.py:503
  51.6 0.2 select_reduce_fusion
  51.8 0.4 convolution_convert_fusion.1
  52.2 0.3 copy-done.14
  52.5 0.4 broadcast_select_fusion.2
  53.0 0.7 copy-done.29
  53.7 0.2 copy-done.30
  53.9 5.8 %fusion.13 = f32[192,1792]{1,0:T(8,128)} fusion(bf16[2048,1792]{1,0:T(8,128)(2,1)} %param.45, bf16[192,1024]{1,0:T(8,128)(2,1)S(1)} %get-tuple-element.17, bf16[192,1024]{1,0:T(8,128)(2,1)S(1)} %get-tuple-element.16), kind=kOutput, calls=%fused_computation.31 | convolution fusion | flops 1410859008 | bytes 9502720 | tf_op jit(solution)/shard_map/dot_general | solution.py:507
  59.7 10.2 %fusion = bf16[192,2048]{1,0:T(8,128)(2,1)} fusion(bf16[1792,2048]{1,0:T(8,128)(2,1)} %param.47, f32[192]{0:T(256)S(1)} %select_reduce_fusion, bf16[2048,1792]{1,0:T(8,128)(2,1)} %param.46, f32[192,1792]{1,0:T(8,128)} %fusion.13, bf16[192,1024]{1,0:T(8,128)(2,1)} %copy-done.30, bf16[192,1024]{1,0:T(8,128)(2,1)} %copy-done.29), kind=kOutput, calls=%fused_computation.2 | convolution fusion | flops 2822995968 | bytes 17629952 | tf_op jit(solution)/shard_map/dot_general | solution.py:507
  69.9 1.8 %fusion.16 = f32[512,1024]{1,0:T(8,128)S(1)} fusion(pred[]{:T(512)S(6)} %eq.56, bf16[192,2048]{1,0:T(8,128)(2,1)} %fusion, f32[512]{0:T(512)S(1)} %eq.53, s32[512]{0:T(512)S(1)} %add_select_fusion, f32[192]{0:T(256)S(1)} %get-tuple-element.29, s32[192]{0:T(256)S(1)} %get-tuple-element.28), kind=kOutput, calls=%fused_computation.34 | convolution fusion | flops 201818112 | bytes 2889217 | tf_op jit(solution)/shard_map/dot_general | solution.py:521
  71.8 1.7 %fusion.14 = f32[512,1024]{1,0:T(8,128)S(1)} fusion(pred[]{:T(512)S(6)} %eq.56, bf16[192,2048]{1,0:T(8,128)(2,1)} %fusion, f32[512]{0:T(512)S(1)} %eq.53, s32[512]{0:T(512)S(1)} %add_select_fusion, f32[192]{0:T(256)S(1)} %get-tuple-element.29, s32[192]{0:T(256)S(1)} %get-tuple-element.28), kind=kOutput, calls=%fused_computation.32 | convolution fusion | flops 201818112 | bytes 2889217 | tf_op jit(solution)/shard_map/dot_general | solution.py:521
  73.5 0.6 fusion.6
  74.1 0.1 copy-done.21
  74.3 1.7 %convolution_add_fusion = f32[512,352]{0,1:T(8,128)S(1)} fusion(f32[512,352]{0,1:T(8,128)S(1)} %fusion.6, bf16[512,1024]{1,0:T(8,128)(2,1)S(1)} %bitcast.50, bf16[1024,352]{0,1:T(8,128)(2,1)} %collective-permute-done), kind=kOutput, calls=%fused_computation.7 | convolution fusion | flops 369278976 | bytes 3211264 | tf_op jit(solution)/shard_map/dot_general | solution.py:507
  76.0 0.1 fusion.20
  76.1 0.5 add_convert_fusion.1
  76.6 1.5 %add_convert_fusion = bf16[512,1024]{1,0:T(8,128)(2,1)S(1)} fusion(f32[512,1024]{1,0:T(8,128)S(1)} %fusion.14, bf16[512,176]{0,1:T(8,128)(2,1)S(1)} %fusion.20, bf16[176,1024]{1,0:T(8,128)(2,1)} %collective-permute-done.1, f32[1024]{0:T(1024)S(1)} %add_divide_fusion), kind=kOutput, calls=%fused_computation.5 | convolution fusion | flops 186122240 | bytes 3690496 | tf_op jit(solution)/shard_map/dot_general | solution.py:507
  78.1 21.5 %collect.1 = bf16[32,1024]{1,0:T(8,128)(2,1)S(1)} custom-call(bf16[16,32,1024]{2,1,0:T(8,128)(2,1)S(1)} %bitcast.43, bf16[16,32,1024]{2,1,0:T(8,128)(2,1)S(1)} %bitcast.45, f32[32,1024]{1,0:T(8,128)S(1)} %get-tuple-element.10.kept), custom_call_target="tpu_custom_call" | custom-call | tf_op jit(solution)/shard_map/collect/pallas_call | solution.py:398
  99.6 0.6 copy.50
  (88 shorter events, 1.2 us)
Async XLA Ops:
  0.6 23.9 %copy-start = (bf16[512,2048]{1,0:T(8,128)(2,1)S(1)}, bf16[512,2048]{1,0:T(8,128)(2,1)}, u32[]{:S(2)}) copy-start(bf16[512,2048]{1,0:T(8,128)(2,1)} %param.41) | copy-start | bytes 6291460
  0.6 73.6 %collective-permute-start.2 = (f32[1024]{0:T(1024)}, f32[1024]{0:T(1024)S(1)}, u32[]{:S(2)}, u32[]{:S(2)}) collective-permute-start(f32[1024]{0:T(1024)} %param.51), channel_id=1, source_target_pairs={{0,1},{1,0},{2,3},{3,2},{4,5},{5,4},{6,7},{7,6},{8,9},{9,8},{10,11... | collective-permute-start | bytes 12296 | tf_op jit(solution)/shard_map/ppermute | solution.py:465
  3.1 3.9 %copy-start.2 = (bf16[32,2048]{1,0:T(8,128)(2,1)S(1)}, bf16[32,2048]{1,0:T(8,128)(2,1)}, u32[]{:S(2)}) copy-start(bf16[32,2048]{1,0:T(8,128)(2,1)} %stream.1) | copy-start | bytes 393220
  3.1 4.0 %copy-start.18 = (f32[2048]{0:T(1024)S(1)}, f32[2048]{0:T(1024)}, u32[]{:S(2)}) copy-start(f32[2048]{0:T(1024)} %param.27) | copy-start | bytes 24580
  3.2 73.5 %collective-permute-start.1 = (bf16[176,1024]{1,0:T(8,128)(2,1)}, bf16[176,1024]{1,0:T(8,128)(2,1)}, u32[]{:S(2)}, u32[]{:S(2)}) collective-permute-start(bf16[176,1024]{1,0:T(8,128)(2,1)} %broadcast_select_fusion.3), channel_id=1, source_target_pairs={{0,1},{1,0},{2,3},{3,2},{4,5},{5,4},{6,7},{7,6},{8,9},{9,8},{10,11... | collective-permute-start | bytes 1081352 | tf_op jit(solution)/shard_map/ppermute | solution.py:464
  4.7 0.7 copy-start.6
  4.7 1.9 %copy-start.8 = (bf16[1024,176]{0,1:T(8,128)(2,1)}, bf16[1024,176]{0,1:T(8,128)(2,1)S(1)}, u32[]{:S(2)}) copy-start(bf16[1024,176]{0,1:T(8,128)(2,1)S(1)} %get-tuple-element.19) | copy-start | bytes 1081348
  4.7 1.9 %copy-start.10 = (bf16[1024,176]{0,1:T(8,128)(2,1)}, bf16[1024,176]{0,1:T(8,128)(2,1)S(1)}, u32[]{:S(2)}) copy-start(bf16[1024,176]{0,1:T(8,128)(2,1)S(1)} %get-tuple-element.30) | copy-start | bytes 1081348
  4.7 1.8 %copy-start.12 = (bf16[1024,176]{0,1:T(8,128)(2,1)}, bf16[1024,176]{0,1:T(8,128)(2,1)S(1)}, u32[]{:S(2)}) copy-start(bf16[1024,176]{0,1:T(8,128)(2,1)S(1)} %get-tuple-element.31) | copy-start | bytes 1081348
  4.7 5.2 %copy-start.27 = (f32[8]{0:T(128)S(1)}, f32[8]{0:T(128)}, u32[]{:S(2)}) copy-start(f32[8]{0:T(128)} %param.33) | copy-start | bytes 100
  4.7 5.2 %copy-start.22 = (s32[32,2]{0,1:T(2,128)S(1)}, s32[32,2]{0,1:T(2,128)}, u32[]{:S(2)}) copy-start(s32[32,2]{0,1:T(2,128)} %param.43) | copy-start | bytes 772
  4.7 5.2 %copy-start.20 = (f32[2,4,128]{2,1,0:T(4,128)S(1)}, f32[2,4,128]{2,1,0:T(4,128)}, u32[]{:S(2)}) copy-start(f32[2,4,128]{2,1,0:T(4,128)} %param.35) | copy-start | bytes 12292
  4.7 5.2 %copy-start.25 = (f32[8]{0:T(128)S(1)}, f32[8]{0:T(128)}, u32[]{:S(2)}) copy-start(f32[8]{0:T(128)} %param.39) | copy-start | bytes 100
  4.8 5.4 %copy-start.24 = (f32[32,2]{0,1:T(2,128)S(1)}, f32[32,2]{0,1:T(2,128)}, u32[]{:S(2)}) copy-start(f32[32,2]{0,1:T(2,128)} %param.44) | copy-start | bytes 772
  4.8 5.4 %copy-start.17 = (bf16[32,2,3,128]{3,1,2,0:T(2,128)(2,1)S(1)}, bf16[32,2,3,128]{3,1,2,0:T(2,128)(2,1)}, u32[]{:S(2)}) copy-start(bf16[32,2,3,128]{3,1,2,0:T(2,128)(2,1)} %param.37) | copy-start | bytes 147460
  5.4 5.0 %copy-start.26 = (bf16[2048,8]{0,1:T(8,128)(2,1)S(1)}, bf16[2048,8]{0,1:T(8,128)(2,1)}, u32[]{:S(2)}) copy-start(bf16[2048,8]{0,1:T(8,128)(2,1)} %param.31) | copy-start | bytes 98308
  5.4 5.0 %copy-start.28 = (f32[8]{0:T(128)S(1)}, f32[8]{0:T(128)}, u32[]{:S(2)}) copy-start(f32[8]{0:T(128)} %param.32) | copy-start | bytes 100
  6.5 67.7 %collective-permute-start = (bf16[1024,352]{0,1:T(8,128)(2,1)}, bf16[1024,352]{0,1:T(8,128)(2,1)}, u32[]{:S(2)}, u32[]{:S(2)}) collective-permute-start(bf16[1024,352]{0,1:T(8,128)(2,1)} %broadcast_select_fusion), channel_id=1, source_target_pairs={{0,1},{1,0},{2,3},{3,2},{4,5},{5,4},{6,7},{7,6},{8,9},{9,8},{10,11... | collective-permute-start | bytes 2162696 | tf_op jit(solution)/shard_map/ppermute | solution.py:462
  8.5 4.8 %copy-start.16 = (bf16[32,3,512]{2,0,1:T(8,128)(2,1)S(1)}, bf16[32,3,512]{2,0,1:T(8,128)(2,1)}, u32[]{:S(2)}) copy-start(bf16[32,3,512]{2,0,1:T(8,128)(2,1)} %param.36) | copy-start | bytes 294916
  8.5 4.8 %copy-start.19 = (f32[4,512]{1,0:T(4,128)S(1)}, f32[4,512]{1,0:T(4,128)}, u32[]{:S(2)}) copy-start(f32[4,512]{1,0:T(4,128)} %param.34) | copy-start | bytes 24580
  13.7 2.2 %copy-start.1 = (f32[32,8,4096]{2,1,0:T(8,128)S(1)}, f32[32,8,4096]{2,1,0:T(8,128)}, u32[]{:S(2)}) copy-start(f32[32,8,4096]{2,1,0:T(8,128)} %param.38) | copy-start | bytes 12582916
  21.7 2.8 %copy-start.23 = (f32[512]{0:T(512)S(1)}, f32[512]{0:T(512)}, u32[]{:S(2)}) copy-start(f32[512]{0:T(512)} %param.40) | copy-start | bytes 6148
  21.8 3.2 %copy-start.4 = (f32[2048]{0:T(1024)S(1)}, f32[2048]{0:T(1024)}, u32[]{:S(2)}) copy-start(f32[2048]{0:T(1024)} %param.42) | copy-start | bytes 24580
  48.2 1.3 %copy-start.3 = (bf16[2,16,32,1024]{3,2,1,0:T(8,128)(2,1)}, bf16[2,16,32,1024]{3,2,1,0:T(8,128)(2,1)S(1)}, u32[]{:S(2)}) copy-start(bf16[2,16,32,1024]{3,2,1,0:T(8,128)(2,1)S(1)} %get-tuple-element.9) | copy-start | bytes 6291460
  51.6 1.0 copy-start.14
  53.0 0.8 copy-start.29
  53.0 0.9 copy-start.30
  69.9 3.6 %copy-start.7 = (bf16[1024,176]{0,1:T(8,128)(2,1)S(1)}, bf16[1024,176]{0,1:T(8,128)(2,1)}, u32[]{:S(2)}) copy-start(bf16[1024,176]{0,1:T(8,128)(2,1)} %copy-done.6) | copy-start | bytes 1081348
  69.9 3.6 %copy-start.9 = (bf16[1024,176]{0,1:T(8,128)(2,1)S(1)}, bf16[1024,176]{0,1:T(8,128)(2,1)}, u32[]{:S(2)}) copy-start(bf16[1024,176]{0,1:T(8,128)(2,1)} %copy-done.8) | copy-start | bytes 1081348
  69.9 3.6 %copy-start.11 = (bf16[1024,176]{0,1:T(8,128)(2,1)S(1)}, bf16[1024,176]{0,1:T(8,128)(2,1)}, u32[]{:S(2)}) copy-start(bf16[1024,176]{0,1:T(8,128)(2,1)} %copy-done.10) | copy-start | bytes 1081348
  69.9 3.6 %copy-start.13 = (bf16[1024,176]{0,1:T(8,128)(2,1)S(1)}, bf16[1024,176]{0,1:T(8,128)(2,1)}, u32[]{:S(2)}) copy-start(bf16[1024,176]{0,1:T(8,128)(2,1)} %copy-done.12) | copy-start | bytes 1081348
  69.9 3.6 %copy-start.15 = (bf16[1,16,32,1024]{3,2,1,0:T(8,128)(2,1)S(1)}, bf16[1,16,32,1024]{3,2,1,0:T(8,128)(2,1)}, u32[]{:S(2)}) copy-start(bf16[1,16,32,1024]{3,2,1,0:T(8,128)(2,1)} %copy-done.14) | copy-start | bytes 3145732
  73.5 0.7 copy-start.21
  74.2 1.9 %copy-start.5 = (bf16[352,1024]{1,0:T(8,128)(2,1)S(1)}, bf16[352,1024]{1,0:T(8,128)(2,1)}, u32[]{:S(2)}) copy-start(bf16[352,1024]{1,0:T(8,128)(2,1)} %param.50) | copy-start | bytes 2162692
where the time goes:
time: 101 us; the launch traced here: 100 us
  Pallas kernels  50.5 us (50%)
  matrix products  32.4 us (32%)
  local copies, waits for them, and re-layouts  10.8 us (11%)
  other arithmetic  4.07 us (4%)
  between operations  1.28 us (1%)
  starting transfers between devices  1.13 us (1%)
    pallas_call x1, Pallas kernels, spread(): pl.pallas_call(functools.partial(spread_kernel, ep_count), out_shape=(jax...  23.2 us
    pallas_call x1, Pallas kernels, collect(): pl.pallas_call(functools.partial(collect_kernel, ep_count), out_shape=jax...  21.5 us
    dot_general x8, matrix products, f32_dot(): return jnp.dot(left, right, preferred_element_type=jnp.float32)  21.1 us
    unnamed x65, local copies, waits for them, and re-layouts  6.22 us
    pallas_call x1, Pallas kernels, step_state(): pl.pallas_call(state_kernel, grid=(flat // rows,), out_shape=(jax.ShapeDt...  5.79 us
    dot_general x2, matrix products, result(): lax.dot_general(pick, share_half, (((0,), (0,)), ((), ())), preferred_ele...  3.53 us
    select_n x2, other arithmetic, mine(): return jnp.where(first, left, right)  3.08 us
    dot_general x1, matrix products, mix_heads(): jnp.dot(normed, gate_proj, preferred_element_type=jnp.float32)  2.13 us
  transfers between devices with their start and end apart: 3, of which 0 were waited for; matrix products, arithmetic and copies ran while one was open for 40% of the time, Pallas kernels for 29%

commit v1 on v0

v1 whole, which is shorter than its diff:
```python
import functools

import jax
import jax.numpy as jnp
from jax import lax
from jax.experimental import pallas as pl
from jax.experimental.pallas import tpu as pltpu
from jax.sharding import PartitionSpec as P

HEAD = 64
HEADS = 16
GROUPS = 4
NSTATE = 64
EXPERTS = 8
TOP_K = 2
CAP = 12
PAST = 3

EPS = 1e-06
MESH = pl.DeviceIdType.MESH
TILE = 256
F32 = jnp.float32
BF16 = jnp.bfloat16
MAPS_LEFT = (((1,), (1,)), ((), ()))


def rms_scale(values):
    return values * lax.rsqrt(jnp.mean(values * values, axis=-1, keepdims=True) + EPS)


def silu(values):
    return values / (1.0 + jnp.exp(-values))


def f32_dot(left, right):
    return jnp.dot(left, right, preferred_element_type=F32)


def dot_by_rows(left, right):
    return lax.dot_general(left, right, MAPS_LEFT, preferred_element_type=F32)


def parts_of(value, count):
    parts = []
    for _ in range(count):
        part = value.astype(BF16)
        parts.append(part)
        value = value - part.astype(F32)
    return parts


def iota(shape, dim):
    return lax.broadcasted_iota(jnp.int32, shape, dim)


def grid_of(ep_count):
    side = 4 if ep_count % 64 == 0 else (2 if ep_count % 4 == 0 else 1)
    return side, ep_count // (side * side)


LOADS = 13


def mix_kernel(ep_count, step_bias, decay_rate, skip_gain, *refs):
    loads, refs = refs[:LOADS], refs[LOADS:]
    (state_in, inner_out, state_out, notes), refs = refs[:4], refs[4:]
    stores, refs = refs[:LOADS], refs[LOADS:]
    held, wide_fed, wide_write, wide_read, wide_decay, total, load_sem, in_sem, out_sem = refs
    copies = []
    for i, (src, dst) in enumerate(zip(loads, stores)):
        copies.append(pltpu.make_async_copy(src, dst, load_sem.at[i]))
        copies[-1].start()
    flat, lanes = held.shape
    tiles = lanes // TILE

    def stripe(t):
        return pl.ds(pl.multiple_of(t * TILE, TILE), TILE)

    for t in range(tiles):
        cut = stripe(t)
        pltpu.make_async_copy(state_in.at[:, cut], held.at[:, cut], in_sem.at[t]).start()

    (
        stream, mixer_gain, ids, weight, gate_proj, input_proj, state_maps, step_proj,
        input_taps, map_taps, input_past, map_past, inner_gain,
    ) = stores
    ready = iter(copies)

    def wait(count):
        for _ in range(count):
            next(ready).wait()

    wait(4)
    row_count = stream.shape[0]
    normed = (rms_scale(stream[...].astype(F32)) * mixer_gain[...]).astype(BF16)

    side, line = grid_of(ep_count)
    place_z = lax.axis_index("ep") // (side * side)
    span = notes.shape[2]
    expert = iota((EXPERTS, row_count), 0)
    named = [ids[k : k + 1, :] == expert for k in range(TOP_K)]
    hits = functools.reduce(jnp.logical_or, named)
    before = iota((row_count, row_count), 0) < iota((row_count, row_count), 1)
    rank = f32_dot(
        jnp.where(hits, 1.0, 0.0).astype(BF16), jnp.where(before, 1.0, 0.0).astype(BF16)
    )
    rank = jnp.where(hits, rank + 1.0, 0.0).astype(BF16)
    share = sum(jnp.where(named[k], weight[k : k + 1, :], 0.0) for k in range(TOP_K))
    lay = iota((row_count, span), 0) + place_z * row_count == iota((row_count, span), 1)
    lay = jnp.where(lay, 1.0, 0.0).astype(BF16)
    rank_out = f32_dot(rank, lay)
    share_out = sum(f32_dot(part, lay) for part in parts_of(share, 3)[::-1])
    for e in range(EXPERTS):
        notes[e, 0:1, :] = rank_out[e : e + 1, :]
        notes[e, 1:2, :] = share_out[e : e + 1, :]

    wait(4)
    gate_in = f32_dot(normed, gate_proj[...]).astype(BF16).astype(F32)
    input_new = f32_dot(normed, input_proj[...]).astype(BF16).astype(F32)
    map_new = [f32_dot(normed, state_maps[m]).astype(BF16).astype(F32) for m in range(2)]
    step = dot_by_rows(normed, step_proj[...])
    wait(5)
    channels = input_new.shape[1]
    conv_in = input_taps[PAST : PAST + 1, :] * input_new
    for t in range(PAST):
        conv_in = conv_in + input_taps[t : t + 1, :] * input_past[t].astype(F32)
    conv_in = silu(conv_in)
    olds = map_past.shape[0]
    sort_to = iota((olds, olds), 0)
    sort_from = iota((olds, olds), 1)
    source = (sort_to % row_count) * (2 * PAST) + sort_to // row_count
    sort = jnp.where(sort_from == source, 1.0, 0.0).astype(BF16)
    sorted_past = f32_dot(sort, map_past[...])
    conv_map = []
    for m in range(2):
        value = map_taps[m, PAST : PAST + 1, :] * map_new[m]
        for t in range(PAST):
            at = (t * 2 + m) * row_count
            value = value + map_taps[m, t : t + 1, :] * sorted_past[at : at + row_count]
        conv_map.append(silu(value))

    heads = flat // row_count
    per_group = HEADS // GROUPS

    def row_of(scalars, width):
        lane = iota((1, heads * width), 1) // width
        return sum(jnp.where(lane == h, scalars[h], 0.0) for h in range(heads))

    step = step + row_of(step_bias, 1)
    step_size = jnp.maximum(step, 0.0) + jnp.log1p(jnp.exp(-jnp.abs(step)))
    decay = jnp.exp(-row_of(decay_rate, 1) * step_size)

    def by_head(values):
        width = values.shape[1]
        wide = jnp.broadcast_to(values[:, None, :], (row_count, heads, width))
        return wide.reshape(flat, width)

    def column(values):
        hit = iota((flat, heads), 0) % heads == iota((flat, heads), 1)
        return jnp.sum(jnp.where(hit, by_head(values), 0.0), axis=1, keepdims=True)

    head = iota((flat, 2 * HEAD), 0) % heads
    half = iota((flat, 2 * HEAD), 1) // HEAD

    def doubled(values, which):
        pair = which // 2
        kept = values[:, : 2 * HEAD]
        for k in range(1, values.shape[1] // (2 * HEAD)):
            kept = jnp.where(pair == k, values[:, 2 * HEAD * k : 2 * HEAD * (k + 1)], kept)
        return jnp.where(half == which % 2, kept, pltpu.roll(kept, HEAD, 1))

    fed = column(step_size) * doubled(by_head(conv_in), head)
    high, middle, low = parts_of(fed, 3)
    zero = jnp.zeros_like(low)
    wide_fed[:, : 2 * HEAD] = jnp.where(half == 0, high, middle)
    wide_fed[:, 2 * HEAD :] = jnp.where(half == 0, low, zero)
    wide_write[...] = doubled(by_head(conv_map[0]), head // per_group)
    wide_read[...] = doubled(by_head(conv_map[1]), head // per_group)
    wide_decay[...] = jnp.broadcast_to(column(decay), wide_decay.shape)
    total[...] = jnp.zeros_like(total)
    repeat = TILE // (2 * HEAD)

    @pl.loop(0, tiles)
    def _(t):
        cut = stripe(t)
        shape = (4 * HEAD, TILE)
        base = t * (TILE // NSTATE)
        pick = iota(shape, 0) % HEAD == iota(shape, 1) // NSTATE + base
        pick = jnp.where(pick, 1.0, 0.0).astype(BF16)
        gather = iota((TILE, 2 * HEAD), 0) // NSTATE + base == iota((TILE, 2 * HEAD), 1) % HEAD
        gather = jnp.where(gather, 1.0, 0.0).astype(BF16)
        pltpu.make_async_copy(held.at[:, cut], held.at[:, cut], in_sem.at[t]).wait()
        spread = f32_dot(wide_fed[...], pick)
        write = jnp.concatenate([wide_write[...]] * repeat, axis=1)
        value = jnp.concatenate([wide_decay[...]] * repeat, axis=1) * held[:, cut]
        value = value + spread * write
        held[:, cut] = value
        pltpu.make_async_copy(held.at[:, cut], state_out.at[:, cut], out_sem.at[t]).start()
        product = value * jnp.concatenate([wide_read[...]] * repeat, axis=1)
        total[...] += sum(f32_dot(part, gather) for part in parts_of(product, 2)[::-1])

    pieces = []
    for k in range(channels // (2 * HEAD)):
        mine = (head // 2 == k) & (half == head % 2)
        piece = jnp.where(mine, total[...], 0.0).reshape(row_count, heads, 2 * HEAD)
        pieces.append(jnp.sum(piece, axis=1))
    gated = jnp.concatenate(pieces, axis=1) + row_of(skip_gain, HEAD) * conv_in
    gated = gated * silu(gate_in)
    group = per_group * HEAD
    for at in range(0, channels, group):
        cut = slice(at, at + group)
        scaled = rms_scale(gated[:, cut]) * inner_gain[:, cut]
        inner_out[:, cut] = scaled.astype(BF16)
    for t in range(tiles):
        cut = stripe(t)
        pltpu.make_async_copy(held.at[:, cut], state_out.at[:, cut], out_sem.at[t]).wait()


def mix_heads(
    stream, mixer_gain, gate_proj, input_proj, state_maps, step_proj, step_bias, decay_rate,
    input_taps, map_taps, input_past, map_past, head_state, skip_gain, inner_gain,
    expert_ids, expert_weight,
):
    ep_count = lax.axis_size("ep")
    side, line = grid_of(ep_count)
    row_count = stream.shape[0]
    heads, lanes = head_state.shape[1:]
    channels = gate_proj.shape[1]
    flat = row_count * heads
    loads = (
        stream, mixer_gain[None, :], expert_ids.T, expert_weight.T,
        gate_proj, input_proj, state_maps, step_proj.T,
        input_taps, map_taps, input_past.transpose(1, 0, 2),
        map_past.transpose(0, 2, 1, 3).reshape(-1, map_past.shape[3]), inner_gain[None, :],
    )
    vmem = pl.BlockSpec(memory_space=pltpu.VMEM)
    smem = pl.BlockSpec(memory_space=pltpu.SMEM)
    any_space = pl.BlockSpec(memory_space=pl.ANY)
    dma = pltpu.SemaphoreType.DMA
    wide = pltpu.VMEM((flat, 2 * HEAD), F32)
    inner, state_new, notes = pl.pallas_call(
        functools.partial(mix_kernel, ep_count),
        out_shape=(
            jax.ShapeDtypeStruct((row_count, channels), BF16),
            jax.ShapeDtypeStruct((flat, lanes), F32),
            jax.ShapeDtypeStruct((EXPERTS, 2, line * row_count), F32),
        ),
        in_specs=[smem] * 3 + [any_space] * (LOADS + 1),
        out_specs=(vmem, any_space, vmem),
        scratch_shapes=[pltpu.VMEM(x.shape, x.dtype) for x in loads] + [
            pltpu.VMEM((flat, lanes), F32),
            pltpu.VMEM((flat, 4 * HEAD), BF16),
            wide, wide, wide, wide,
            dma((LOADS,)), dma((lanes // TILE,)), dma((lanes // TILE,)),
        ],
        compiler_params=pltpu.CompilerParams(vmem_limit_bytes=60 * 1024 * 1024),
        name="mix",
    )(step_bias, decay_rate, skip_gain, *loads, head_state.reshape(flat, lanes))
    return inner, state_new.reshape(row_count, heads, lanes), notes


class Place:
    def __init__(self, ep_count):
        self.side, self.line = grid_of(ep_count)
        self.ep = lax.axis_index("ep")
        self.core = lax.axis_index("tp")
        self.col = self.ep % self.side
        self.row = (self.ep // self.side) % self.side
        self.z = self.ep // (self.side * self.side)

    def ahead(self, db, da, core=None):
        core = self.core if core is None else core
        a = (self.row * (1 - core) + self.col * core + da) % self.side
        b = (self.col * (1 - core) + self.row * core + db) % self.side
        return a * (1 - core) + b * core, b * (1 - core) + a * core

    def near(self, db, da, dz):
        row, col = self.ahead(db, da)
        z = (self.z + dz) % self.line
        return {"ep": (z * self.side + row) * self.side + col, "tp": self.core}

    def plane(self, db, da):
        row, col = self.ahead(db, da)
        return row * self.side + col

    def spot(self, db, da, dz):
        return self.plane(db, da) * self.line + (self.z + dz) % self.line

    def sibling(self):
        return {"ep": self.ep, "tp": 1 - self.core}

    def z_order(self):
        line = self.line
        return sorted(range(1, line), key=lambda d: (min(d, line - d), d))


def greet(targets):
    barrier = pltpu.get_barrier_semaphore()
    for target in targets:
        pl.semaphore_signal(barrier, inc=1, device_id=target, device_id_type=MESH)
    return lambda: pl.semaphore_wait(barrier, len(targets))


def ffn_kernel(ep_count, *refs):
    (
        inner, stream, gain, notes_in, mix, mixer_out, dense_gate, dense_up, dense_down,
        expert_gate, expert_up, expert_down, out,
        out_w, gate_w, up_w, down_w, wide_gate, wide_up, wide_down,
        partial, other, hidden, every, notes, acts, rows, act, dense, own, give, take, share,
        total, from_b, from_a, from_z,
        load_sem, swap_sem, note_send, note_recv, link_send, link_recv, core_send, core_recv,
        weight_sem, act_send, act_recv, give_sem, sum_send, recv_b, recv_a, recv_z,
    ) = refs
    place = Place(ep_count)
    side, line = place.side, place.line
    core, me = place.core, place.ep
    row_count, width = stream.shape
    half = width // 2
    units = dense_gate.shape[0]
    part = row_count // 2
    span = line * row_count
    slots = line * CAP
    my_rows = pl.ds(pl.multiple_of(core * part, part), part)
    my_half = pl.ds(pl.multiple_of(core * half, half), half)
    everyone = [{"ep": (me + d) % ep_count, "tp": core} for d in range(1, ep_count)]
    greeted = greet([place.sibling()] + everyone)
    sends = []

    def load(at, src, dst):
        copy = pltpu.make_async_copy(src, dst, load_sem.at[at])
        copy.start()
        return copy

    def send(src, dst, send_sem, recv_sem, target):
        copy = pltpu.make_async_remote_copy(
            src_ref=src, dst_ref=dst, send_sem=send_sem, recv_sem=recv_sem,
            device_id=target, device_id_type=MESH,
        )
        copy.start()
        sends.append(copy)
        return copy

    def landed(ref, sem):
        pltpu.make_async_copy(ref, ref, sem).wait()

    out_load = load(0, mixer_out, out_w)
    dense_loads = [
        load(1, dense_gate, gate_w.at[core]),
        load(2, dense_up, up_w.at[core]),
        load(3, dense_down, down_w),
    ]
    out_load.wait()
    partial[...] = f32_dot(inner[...], out_w[...]).astype(BF16)
    expert_loads = [
        load(4, expert_gate, wide_gate), load(5, expert_up, wide_up),
        load(6, expert_down, wide_down),
    ]
    greeted()
    swap = send(partial, other, swap_sem.at[0], swap_sem.at[1], place.sibling())
    here = place.spot(0, 0, 0)
    for d in range(1, ep_count):
        target = (me + d) % ep_count
        expert = target // (ep_count // EXPERTS)
        send(
            notes_in.at[expert], notes.at[here], note_send.at[d - 1], note_recv.at[d - 1],
            everyone[d - 1],
        )
    notes[here] = notes_in[me // (ep_count // EXPERTS)]
    swap.wait_recv()
    middle = stream[...].astype(F32) + (partial[...].astype(F32) + other[...].astype(F32))
    hidden[...] = middle
    every[here] = (rms_scale(middle) * gain[...]).astype(BF16)

    def slot(db, da, dz):
        return ((db % side) * side + da % side) * line + dz % line

    def block(off):
        return every.at[place.spot(*off), my_rows]

    used = [0]

    def pass_on(off, step):
        there = slot(*(o - s for o, s in zip(off, step)))
        send(
            block(off), block(off), link_send.at[used[0]], link_recv.at[there], place.near(*step)
        )
        used[0] += 1

    def arrived(off):
        at = slot(*off)
        landed(block(off), link_recv.at[at])
        send(block(off), block(off), core_send.at[at], core_recv.at[at], place.sibling())

    zs = [0] + place.z_order()
    for dz in zs[1:]:
        pass_on((0, 0, 0), (0, 0, dz))
    for i, (src, dst) in enumerate(((dense_gate, gate_w), (dense_up, up_w))):
        send(
            src, dst.at[core], weight_sem.at[2 * i], weight_sem.at[2 * i + 1], place.sibling()
        )
    for dz in zs:
        if dz:
            arrived((0, 0, dz))
        for d in range(1, side):
            pass_on((0, 0, dz), (0, d, 0))
        for d in range(1, side):
            pass_on((0, 0, dz), (d, 0, 0))
    for dz in zs:
        for da in range(1, side):
            arrived((0, da, dz))
            for d in range(1, side):
                pass_on((0, da, dz), (d, 0, 0))

    def planes_of(db):
        return [(db, da) for da in range(side)]

    def group(at, size):
        return pl.ds(pl.multiple_of(at * size, size), size)

    for i, dst in enumerate((gate_w, up_w)):
        dense_loads[i].wait()
        landed(dst.at[1 - core], weight_sem.at[2 * i + 1])

    def dense_in(planes):
        tall = len(planes) * line * part
        seen = jnp.concatenate(
            [every[group(place.plane(*at), line), my_rows].reshape(-1, width) for at in planes],
            axis=0,
        )

        def product(weights):
            return dot_by_rows(seen[:, :half], weights[0]) + dot_by_rows(
                seen[:, half:], weights[1]
            )

        value = (silu(product(gate_w)) * product(up_w)).astype(BF16)
        value = value.reshape(len(planes), line, part, units)
        for i, at in enumerate(planes):
            theirs = acts.at[group(place.plane(*at), line), my_rows]
            acts[group(place.plane(*at), line), my_rows] = value[i]
            k = at[0] * side + at[1]
            send(theirs, theirs, act_send.at[k], act_recv.at[k], place.sibling())

    dense_in(planes_of(0))
    for dz in zs:
        for da in range(side):
            for db in range(1, side):
                arrived((db, da, dz))
    for db in range(1, side):
        dense_in(planes_of(db))
    for d in range(1, ep_count):
        source = (me + ep_count - d) % ep_count
        at = (source % (side * side)) * line + source // (side * side)
        landed(notes.at[at], note_recv.at[d - 1])

    def matches(at):
        info = notes[group(at, line)].sum(axis=0)
        slot_id = iota((slots, span), 0)
        row_id = iota((slots, span), 1)
        hit = (slot_id // CAP == row_id // row_count) & (
            (slot_id % CAP + 1).astype(F32) == info[0:1]
        )
        return hit, info[1:2]

    planes = [(db, da) for db in range(side) for da in range(side)]
    for db, da in planes:
        at = place.plane(db, da)
        for dz in zs:
            if db or da or dz:
                theirs = every.at[place.spot(db, da, dz), other_rows(core, part)]
                landed(theirs, core_recv.at[slot(da, db, dz)])
        hit, _ = matches(at)
        pick = jnp.where(hit, 1.0, 0.0).astype(BF16)
        seen = every[group(at, line)].reshape(span, width)
        rows[group(at, slots), :] = f32_dot(pick, seen).astype(BF16)

    for copy in expert_loads:
        copy.wait()
    deep = expert_gate.shape[1]
    for at in range(0, deep, TILE):
        cut = slice(at, min(at + TILE, deep))
        gated = silu(f32_dot(rows[...], wide_gate[:, cut]))
        act[:, cut] = (gated * f32_dot(rows[...], wide_up[:, cut])).astype(BF16)
    scale = []
    for at in range(side * side):
        hit, weight = matches(at)
        scale.append(jnp.sum(jnp.where(hit, weight, 0.0), axis=1, keepdims=True))
    scale = jnp.concatenate(scale, axis=0)

    def results(first, at):
        cut = pl.ds(pl.multiple_of(first * half + at, TILE), TILE)
        return f32_dot(act[...], wide_down[:, cut]) * scale

    for at in range(0, half, TILE):
        give[:, at : at + TILE] = results(1 - core, at).astype(BF16)
    send(give, take, give_sem.at[0], give_sem.at[1], place.sibling())
    for at in range(0, half, TILE):
        own[:, at : at + TILE] = results(core, at)

    dense_loads[2].wait()
    mixed = jax.nn.sigmoid(mix[...])

    def dense_out(db, da):
        at = place.plane(db, da)
        theirs = acts.at[group(at, line), other_rows(core, part)]
        landed(theirs, act_recv.at[da * side + db])
        seen = acts[group(at, line)].reshape(span, units)
        dense[group(at, span), :] = f32_dot(seen, down_w[...]) * mixed

    for db in range(1, side):
        for da in range(side):
            dense_out(db, da)
    landed(take, give_sem.at[1])
    share[...] = (own[...] + take[...].astype(F32)).astype(BF16)

    def result(db, da):
        at = place.plane(db, da)
        hit, _ = matches(at)
        pick = jnp.where(hit, 1.0, 0.0).T.astype(BF16)
        back = f32_dot(pick, share[group(at, slots), :])
        dense[group(at, span), :] = dense[group(at, span), :] + back

    order = place.z_order() + [0]
    used[0] = 0

    def block_of(off):
        return dense[group(place.spot(*off), row_count), :]

    def give_to(value, dst, sem, step):
        at = used[0]
        used[0] += 1
        total[at] = value.astype(BF16)
        send(total.at[at], dst, sum_send.at[at], sem, place.near(*step))

    def add(value, ref, sem):
        landed(ref, sem)
        return value + ref[...].astype(F32)

    for da in list(range(1, side)) + [0]:
        for db in range(1, side):
            result(db, da)
            for dz in order:
                give_to(
                    block_of((db, da, dz)), from_b.at[db - 1, da, dz], recv_b.at[db - 1, da, dz],
                    (db, 0, 0),
                )
    for da in list(range(1, side)) + [0]:
        dense_out(0, da)
        result(0, da)
        for dz in order:
            value = block_of((0, da, dz))
            for d in range(1, side):
                value = add(value, from_b.at[d - 1, da, dz], recv_b.at[d - 1, da, dz])
            if da:
                give_to(value, from_a.at[da - 1, dz], recv_a.at[da - 1, dz], (0, da, 0))
                continue
            for d in range(1, side):
                value = add(value, from_a.at[d - 1, dz], recv_a.at[d - 1, dz])
            if dz:
                give_to(value, from_z.at[dz - 1], recv_z.at[dz - 1], (0, 0, dz))
                continue
            for d in range(1, line):
                value = add(value, from_z.at[d - 1], recv_z.at[d - 1])
            out[...] = (hidden[:, my_half] + value).astype(out.dtype)
    for copy in sends:
        copy.wait_send()


def other_rows(core, part):
    return pl.ds(pl.multiple_of((1 - core) * part, part), part)


def ffn(
    inner, stream, gain, notes, mix, mixer_out, dense_gate, dense_up, dense_down,
    expert_gate, expert_up, expert_down,
):
    ep_count = lax.axis_size("ep")
    side, line = grid_of(ep_count)
    row_count, width = stream.shape
    half = width // 2
    units = dense_gate.shape[0]
    deep = expert_gate.shape[1]
    slots = ep_count * CAP
    more = max(side - 1, 1)
    block = (row_count, half)
    vmem = pl.BlockSpec(memory_space=pltpu.VMEM)
    any_space = pl.BlockSpec(memory_space=pl.ANY)
    dma = pltpu.SemaphoreType.DMA

    def half_words(*shape):
        return pltpu.VMEM(shape, BF16)

    def words(*shape):
        return pltpu.VMEM(shape, F32)

    return pl.pallas_call(
        functools.partial(ffn_kernel, ep_count),
        out_shape=jax.ShapeDtypeStruct(block, BF16),
        in_specs=[vmem] * 5 + [any_space] * 7,
        out_specs=vmem,
        scratch_shapes=[
            half_words(*mixer_out.shape),
            half_words(2, units, half), half_words(2, units, half), half_words(units, half),
            half_words(width, deep), half_words(width, deep), half_words(deep, width),
            half_words(row_count, width), half_words(row_count, width), words(row_count, width),
            half_words(ep_count, row_count, width), words((ep_count), *notes.shape[1:]),
            half_words(ep_count, row_count, units),
            half_words(slots, width), half_words(slots, deep),
            words(ep_count * row_count, half),
            words(slots, half), half_words(slots, half), half_words(slots, half),
            half_words(slots, half),
            half_words(ep_count, *block), half_words(more, side, line, *block),
            half_words(more, line, *block), half_words(max(line - 1, 1), *block),
            dma((7,)), dma((2,)), dma((ep_count,)), dma((ep_count,)),
            dma((ep_count,)), dma((ep_count,)), dma((ep_count,)), dma((ep_count,)),
            dma((4,)), dma((side * side,)), dma((side * side,)), dma((2,)),
            dma((ep_count,)), dma((more, side, line)), dma((more, line)),
            dma((max(line - 1, 1),)),
        ],
        compiler_params=pltpu.CompilerParams(
            collective_id=1, has_side_effects=True, vmem_limit_bytes=60 * 1024 * 1024
        ),
        name="ffn",
    )(
        inner, stream, gain, notes, mix, mixer_out, dense_gate, dense_up, dense_down,
        expert_gate, expert_up, expert_down,
    )


def local(
    stream, mixer_gain, gate_proj, input_proj, state_maps, step_proj, step_bias, decay_rate,
    input_taps, map_taps, input_past, map_past, head_state, skip_gain, inner_gain, mixer_out,
    channel_gain, expert_ids, expert_weight, expert_gate, expert_up, expert_down,
    dense_gate, dense_up, dense_down, dense_mix,
):
    inner, state_out, notes = mix_heads(
        stream, mixer_gain, gate_proj, input_proj, state_maps, step_proj, step_bias, decay_rate,
        input_taps, map_taps, input_past, map_past, head_state, skip_gain, inner_gain,
        expert_ids, expert_weight,
    )
    updated = ffn(
        inner, stream, channel_gain[None, :], notes, dense_mix[None, :], mixer_out,
        dense_gate.T, dense_up.T, dense_down, expert_gate, expert_up, expert_down,
    )
    return (updated, state_out)


def solution(mesh):
    placed = (
        P("ep", None),
        P(),
        P(None, "tp"),
        P(None, "tp"),
        P(None, None, "tp"),
        P(None, "tp"),
        P("tp"),
        P("tp"),
        P(None, "tp"),
        P(None, None, "tp"),
        P("ep", None, "tp"),
        P("ep", None, None, "tp"),
        P("ep", "tp", None),
        P("tp"),
        P("tp"),
        P("tp", None),
        P(),
        P("ep", None),
        P("ep", None),
        P(None, ("ep", "tp")),
        P(None, ("ep", "tp")),
        P(("ep", "tp"), None),
        P("tp", "ep"),
        P("tp", "ep"),
        P("ep", "tp"),
        P("tp"),
    )
    return jax.shard_map(
        local,
        mesh=mesh,
        in_specs=placed,
        out_specs=(P("ep", "tp"), P("ep", "tp", None)),
        check_vma=False,
    )
```

time: 101 us -> 65.3 us (0.65)
  matrix products: 32.4 us -> 0 us
  Pallas kernels: 50.5 us -> 62.9 us
  local copies, waits for them, and re-layouts: 10.8 us -> 1.47 us
  other arithmetic: 4.07 us -> 0 us
  starting transfers between devices: 1.13 us -> 0 us
    dot_general x17 -> x0, matrix products: 32.4 us -> none  [the longest x8 21.1 us: f32_dot(): return jnp.dot(left, right, preferred_element_type=jnp.float32)]
    pallas_call x3 -> x2, Pallas kernels: 50.5 us -> 62.9 us  [the longest x1 48.7 us: ffn(): pl.pallas_call(functools.partial(ffn_kernel, ep_count), out_shape=jax.Sha...]
    unnamed x65 -> x1, local copies, waits for them, and re-layouts: 6.22 us -> 1.47 us
    slice x4 -> x0, local copies, waits for them, and re-layouts: 3.3 us -> none  [the longest x1 1.73 us: local(): all_own = every[0].reshape(total_rows, half)]
    select_n x4 -> x0, other arithmetic: 3.09 us -> none  [the longest x2 3.08 us: mine(): return jnp.where(first, left, right)]
    ppermute x3 -> x0, starting transfers between devices: 1.13 us -> none  [the longest x1 0.56 us: local(): mix_other = lax.ppermute(dense_mix, 'tp', swap)]
  transfers between devices with their start and end apart: 3 -> 0, of which waited for: 0 -> 0; matrix products, arithmetic and copies ran while one was open for 40% -> 0% of each run, Pallas kernels for 29% -> 0%
where the time goes in v1:
time: 65.3 us; the launch traced here: 65.1 us
  Pallas kernels  62.9 us (96%)
  local copies, waits for them, and re-layouts  1.47 us (2%)
    pallas_call x1, Pallas kernels, ffn(): pl.pallas_call(functools.partial(ffn_kernel, ep_count), out_shape=jax.Sha...  48.7 us
    pallas_call x1, Pallas kernels, mix_heads(): pl.pallas_call(functools.partial(mix_kernel, ep_count), out_shape=(jax.Sh...  14.2 us
    unnamed x1, local copies, waits for them, and re-layouts  1.47 us

profile of v1, /device:TPU:0, one launch (start us, length us, event | category | flops | bytes accessed | tf_op | source)
XLA Modules:
  0.0 65.1 jit_solution(17110406111571838804)
XLA Ops:
  0.6 14.2 %mix.1 = (bf16[32,512]{1,0:T(8,128)(2,1)}, f32[256,4096]{1,0:T(8,128)}, f32[8,2,128]{2,1,0:T(2,128)}) custom-call(f32[8]{0:T(128)} %step_bias.1, f32[8]{0:T(128)} %decay_rate.1, f32[8]{0:T(128)} %skip_gain.1, bf16[32,2048]{1,0:T(8,128)(2,1)} %refs_1_.1, f32[1,2048]{1,0:T(1,128)} %bitcast.22, s32[2,32]{1,0:T(2,128)} %bitcast.25, f32[2,32]{1,0:T(2,128)} %bitcast.26, ...), custom_call_target="tpu_custom_call" | custom-call | tf_op jit(solution)/shard_map/mix/pallas_call | solution.py:241
  14.9 48.7 %ffn.1 = bf16[32,1024]{1,0:T(8,128)(2,1)} custom-call(bf16[32,512]{1,0:T(8,128)(2,1)} %get-tuple-element.5.refs_0_, bf16[32,2048]{1,0:T(8,128)(2,1)} %refs_1_.1, f32[1,2048]{1,0:T(1,128)} %bitcast.21, f32[8,2,128]{2,1,0:T(2,128)} %get-tuple-element.6.refs_3_, f32[1,1024]{1,0:T(1,128)} %bitcast.23, bf16[512,2048]{1,0:T(8,128)(2,1)} %refs_5_.3, ...), custom_call_target="tpu_custom_call" | custom-call | tf_op jit(solution)/shard_map/ffn/pallas_call | solution.py:596
  63.6 1.5 %copy.29 = bf16[32,1024]{1,0:T(8,128)(2,1)} copy(bf16[32,1024]{1,0:T(8,128)(2,1)} %ffn.1) | data formatting | bytes 131072

commit v2 on v1

--- a/solution.py
+++ b/solution.py
@@ -19,6 +19,9 @@
 EPS = 1e-06
 MESH = pl.DeviceIdType.MESH
 TILE = 256
+STRAIGHT_OUT = 1
+STRAIGHT_BACK = 1
+CHUNK = 4 * TILE
 F32 = jnp.float32
 BF16 = jnp.bfloat16
 MAPS_LEFT = (((1,), (1,)), ((), ()))
@@ -58,31 +61,42 @@
     return side, ep_count // (side * side)
 
 
-LOADS = 13
-
-
-def mix_kernel(ep_count, step_bias, decay_rate, skip_gain, *refs):
+LOADS = 14
+
+
+def mix_kernel(step_bias, decay_rate, skip_gain, *refs):
     loads, refs = refs[:LOADS], refs[LOADS:]
-    (state_in, inner_out, state_out, notes), refs = refs[:4], refs[4:]
+    (state_in, partial, state_out, note), refs = refs[:4], refs[4:]
     stores, refs = refs[:LOADS], refs[LOADS:]
-    held, wide_fed, wide_write, wide_read, wide_decay, total, load_sem, in_sem, out_sem = refs
+    inner, held, wide_fed, wide_write, wide_read, wide_decay, total = refs[:7]
+    picks, gathers, load_sem, in_sem, out_sem = refs[7:]
     copies = []
     for i, (src, dst) in enumerate(zip(loads, stores)):
         copies.append(pltpu.make_async_copy(src, dst, load_sem.at[i]))
-        copies[-1].start()
+        if i < LOADS - 1:
+            copies[-1].start()
     flat, lanes = held.shape
     tiles = lanes // TILE
 
     def stripe(t):
         return pl.ds(pl.multiple_of(t * TILE, TILE), TILE)
 
-    for t in range(tiles):
-        cut = stripe(t)
-        pltpu.make_async_copy(state_in.at[:, cut], held.at[:, cut], in_sem.at[t]).start()
+    def chunk(c):
+        return pl.ds(pl.multiple_of(c * CHUNK, CHUNK), CHUNK)
+
+    @pl.loop(0, tiles)
+    def _(t):
+        base = t * (TILE // NSTATE)
+        shape = (4 * HEAD, TILE)
+        pick = iota(shape, 0) % HEAD - iota(shape, 1) // NSTATE == base
+        picks[:, stripe(t)] = jnp.where(pick, 1.0, 0.0).astype(BF16)
+        shape = (TILE, 2 * HEAD)
+        gather = iota(shape, 1) % HEAD - iota(shape, 0) // NSTATE == base
+        gathers[stripe(t), :] = jnp.where(gather, 1.0, 0.0)
 
     (
         stream, mixer_gain, ids, weight, gate_proj, input_proj, state_maps, step_proj,
-        input_taps, map_taps, input_past, map_past, inner_gain,
+        input_taps, map_taps, input_past, map_past, inner_gain, mixer_out,
     ) = stores
     ready = iter(copies)
 
@@ -91,28 +105,15 @@
             next(ready).wait()
 
     wait(4)
+    for c in range(lanes // CHUNK):
+        pltpu.make_async_copy(state_in.at[:, chunk(c)], held.at[:, chunk(c)], in_sem.at[c]).start()
+    copies[-1].start()
     row_count = stream.shape[0]
     normed = (rms_scale(stream[...].astype(F32)) * mixer_gain[...]).astype(BF16)
 
-    side, line = grid_of(ep_count)
-    place_z = lax.axis_index("ep") // (side * side)
-    span = notes.shape[2]
-    expert = iota((EXPERTS, row_count), 0)
-    named = [ids[k : k + 1, :] == expert for k in range(TOP_K)]
-    hits = functools.reduce(jnp.logical_or, named)
-    before = iota((row_count, row_count), 0) < iota((row_count, row_count), 1)
-    rank = f32_dot(
-        jnp.where(hits, 1.0, 0.0).astype(BF16), jnp.where(before, 1.0, 0.0).astype(BF16)
-    )
-    rank = jnp.where(hits, rank + 1.0, 0.0).astype(BF16)
-    share = sum(jnp.where(named[k], weight[k : k + 1, :], 0.0) for k in range(TOP_K))
-    lay = iota((row_count, span), 0) + place_z * row_count == iota((row_count, span), 1)
-    lay = jnp.where(lay, 1.0, 0.0).astype(BF16)
-    rank_out = f32_dot(rank, lay)
-    share_out = sum(f32_dot(part, lay) for part in parts_of(share, 3)[::-1])
-    for e in range(EXPERTS):
-        notes[e, 0:1, :] = rank_out[e : e + 1, :]
-        notes[e, 1:2, :] = share_out[e : e + 1, :]
+    note[...] = jnp.zeros_like(note)
+    note[:TOP_K, :row_count] = weight[...]
+    note[TOP_K:, :row_count] = ids[...].astype(F32)
 
     wait(4)
     gate_in = f32_dot(normed, gate_proj[...]).astype(BF16).astype(F32)
@@ -177,27 +178,22 @@
     wide_write[...] = doubled(by_head(conv_map[0]), head // per_group)
     wide_read[...] = doubled(by_head(conv_map[1]), head // per_group)
     wide_decay[...] = jnp.broadcast_to(column(decay), wide_decay.shape)
-    total[...] = jnp.zeros_like(total)
     repeat = TILE // (2 * HEAD)
 
-    @pl.loop(0, tiles)
-    def _(t):
-        cut = stripe(t)
-        shape = (4 * HEAD, TILE)
-        base = t * (TILE // NSTATE)
-        pick = iota(shape, 0) % HEAD == iota(shape, 1) // NSTATE + base
-        pick = jnp.where(pick, 1.0, 0.0).astype(BF16)
-        gather = iota((TILE, 2 * HEAD), 0) // NSTATE + base == iota((TILE, 2 * HEAD), 1) % HEAD
-        gather = jnp.where(gather, 1.0, 0.0).astype(BF16)
-        pltpu.make_async_copy(held.at[:, cut], held.at[:, cut], in_sem.at[t]).wait()
-        spread = f32_dot(wide_fed[...], pick)
-        write = jnp.concatenate([wide_write[...]] * repeat, axis=1)
-        value = jnp.concatenate([wide_decay[...]] * repeat, axis=1) * held[:, cut]
-        value = value + spread * write
-        held[:, cut] = value
-        pltpu.make_async_copy(held.at[:, cut], state_out.at[:, cut], out_sem.at[t]).start()
-        product = value * jnp.concatenate([wide_read[...]] * repeat, axis=1)
-        total[...] += sum(f32_dot(part, gather) for part in parts_of(product, 2)[::-1])
+    write = jnp.concatenate([wide_write[...]] * repeat, axis=1)
+    read = jnp.concatenate([wide_read[...]] * repeat, axis=1)
+    decay_now = jnp.concatenate([wide_decay[...]] * repeat, axis=1)
+    sums = []
+    for c in range(lanes // CHUNK):
+        cut = chunk(c)
+        pltpu.make_async_copy(held.at[:, cut], held.at[:, cut], in_sem.at[c]).wait()
+        for at in range(c * CHUNK, (c + 1) * CHUNK, TILE):
+            at = slice(at, at + TILE)
+            value = decay_now * held[:, at] + f32_dot(wide_fed[...], picks[:, at]) * write
+            held[:, at] = value
+            sums.append(f32_dot(value * read, gathers[at]))
+        pltpu.make_async_copy(held.at[:, cut], state_out.at[:, cut], out_sem.at[c]).start()
+    total[...] = sum(sums)
 
     pieces = []
     for k in range(channels // (2 * HEAD)):
@@ -210,19 +206,19 @@
     for at in range(0, channels, group):
         cut = slice(at, at + group)
         scaled = rms_scale(gated[:, cut]) * inner_gain[:, cut]
-        inner_out[:, cut] = scaled.astype(BF16)
-    for t in range(tiles):
-        cut = stripe(t)
-        pltpu.make_async_copy(held.at[:, cut], state_out.at[:, cut], out_sem.at[t]).wait()
+        inner[:, cut] = scaled.astype(BF16)
+    wait(1)
+    partial[...] = f32_dot(inner[...], mixer_out[...]).astype(BF16)
+    for c in range(lanes // CHUNK):
+        cut = chunk(c)
+        pltpu.make_async_copy(held.at[:, cut], state_out.at[:, cut], out_sem.at[c]).wait()
 
 
 def mix_heads(
     stream, mixer_gain, gate_proj, input_proj, state_maps, step_proj, step_bias, decay_rate,
     input_taps, map_taps, input_past, map_past, head_state, skip_gain, inner_gain,
-    expert_ids, expert_weight,
+    expert_ids, expert_weight, mixer_out,
 ):
-    ep_count = lax.axis_size("ep")
-    side, line = grid_of(ep_count)
     row_count = stream.shape[0]
     heads, lanes = head_state.shape[1:]
     channels = gate_proj.shape[1]
@@ -231,32 +227,34 @@
         stream, mixer_gain[None, :], expert_ids.T, expert_weight.T,
         gate_proj, input_proj, state_maps, step_proj.T,
         input_taps, map_taps, input_past.transpose(1, 0, 2),
-        map_past.transpose(0, 2, 1, 3).reshape(-1, map_past.shape[3]), inner_gain[None, :],
+        map_past.transpose(0, 2, 1, 3).reshape(-1, map_past.shape[3]), inner_gain[None, :], mixer_out,
     )
     vmem = pl.BlockSpec(memory_space=pltpu.VMEM)
     smem = pl.BlockSpec(memory_space=pltpu.SMEM)
     any_space = pl.BlockSpec(memory_space=pl.ANY)
     dma = pltpu.SemaphoreType.DMA
     wide = pltpu.VMEM((flat, 2 * HEAD), F32)
-    inner, state_new, notes = pl.pallas_call(
-        functools.partial(mix_kernel, ep_count),
+    partial, state_new, note = pl.pallas_call(
+        mix_kernel,
         out_shape=(
-            jax.ShapeDtypeStruct((row_count, channels), BF16),
+            jax.ShapeDtypeStruct((row_count, mixer_out.shape[1]), BF16),
             jax.ShapeDtypeStruct((flat, lanes), F32),
-            jax.ShapeDtypeStruct((EXPERTS, 2, line * row_count), F32),
+            jax.ShapeDtypeStruct((2 * TOP_K, -(-row_count // 128) * 128), F32),
         ),
         in_specs=[smem] * 3 + [any_space] * (LOADS + 1),
         out_specs=(vmem, any_space, vmem),
         scratch_shapes=[pltpu.VMEM(x.shape, x.dtype) for x in loads] + [
+            pltpu.VMEM((row_count, channels), BF16),
             pltpu.VMEM((flat, lanes), F32),
             pltpu.VMEM((flat, 4 * HEAD), BF16),
             wide, wide, wide, wide,
-            dma((LOADS,)), dma((lanes // TILE,)), dma((lanes // TILE,)),
+            pltpu.VMEM((4 * HEAD, lanes), BF16), pltpu.VMEM((lanes, 2 * HEAD), F32),
+            dma((LOADS,)), dma((lanes // CHUNK,)), dma((lanes // CHUNK,)),
         ],
         compiler_params=pltpu.CompilerParams(vmem_limit_bytes=60 * 1024 * 1024),
         name="mix",
     )(step_bias, decay_rate, skip_gain, *loads, head_state.reshape(flat, lanes))
-    return inner, state_new.reshape(row_count, heads, lanes), notes
+    return partial, state_new.reshape(row_count, heads, lanes), note
 
 
 class Place:
@@ -283,6 +281,14 @@
         row, col = self.ahead(db, da)
         return row * self.side + col
 
+    def partners(self):
+        side = range(1, self.side)
+        return (
+            [self.near(db, da, 0) for db in range(self.side) for da in side]
+            + [self.near(d, 0, 0) for d in side]
+            + [self.near(0, 0, d) for d in range(1, self.line)]
+        )
+
     def spot(self, db, da, dz):
         return self.plane(db, da) * self.line + (self.z + dz) % self.line
 
@@ -290,8 +296,14 @@
         return {"ep": self.ep, "tp": 1 - self.core}
 
     def z_order(self):
-        line = self.line
-        return sorted(range(1, line), key=lambda d: (min(d, line - d), d))
+        last = self.line - 1
+        up = (2 * self.z < self.line).astype(jnp.int32)
+        at = self.z * up + (last - self.z) * (1 - up)
+        order = []
+        for i in range(last):
+            to = i + (at <= i).astype(jnp.int32)
+            order.append(((2 * up - 1) * (to - at)) % self.line)
+        return order
 
 
 def greet(targets):
@@ -303,13 +315,13 @@
 
 def ffn_kernel(ep_count, *refs):
     (
-        inner, stream, gain, notes_in, mix, mixer_out, dense_gate, dense_up, dense_down,
+        partial_in, stream_in, gain_in, note_in, mix_in, dense_gate, dense_up, dense_down,
         expert_gate, expert_up, expert_down, out,
-        out_w, gate_w, up_w, down_w, wide_gate, wide_up, wide_down,
+        stream, gain, mix, info, gate_w, up_w, down_w, wide_gate, wide_up, wide_down,
         partial, other, hidden, every, notes, acts, rows, act, dense, own, give, take, share,
-        total, from_b, from_a, from_z,
+        total, from_b, from_a, from_z, from_d,
         load_sem, swap_sem, note_send, note_recv, link_send, link_recv, core_send, core_recv,
-        weight_sem, act_send, act_recv, give_sem, sum_send, recv_b, recv_a, recv_z,
+        weight_sem, act_send, act_recv, give_sem, sum_send, recv_b, recv_a, recv_z, recv_d,
     ) = refs
     place = Place(ep_count)
     side, line = place.side, place.line
@@ -322,8 +334,7 @@
     slots = line * CAP
     my_rows = pl.ds(pl.multiple_of(core * part, part), part)
     my_half = pl.ds(pl.multiple_of(core * half, half), half)
-    everyone = [{"ep": (me + d) % ep_count, "tp": core} for d in range(1, ep_count)]
-    greeted = greet([place.sibling()] + everyone)
+    greeted = greet([place.sibling()] + place.partners())
     sends = []
 
     def load(at, src, dst):
@@ -343,29 +354,24 @@
     def landed(ref, sem):
         pltpu.make_async_copy(ref, ref, sem).wait()
 
-    out_load = load(0, mixer_out, out_w)
+    here = place.spot(0, 0, 0)
+    first_loads = [
+        load(0, partial_in, partial), load(1, stream_in, stream), load(2, gain_in, gain),
+        load(3, note_in, notes.at[here]),
+    ]
     dense_loads = [
-        load(1, dense_gate, gate_w.at[core]),
-        load(2, dense_up, up_w.at[core]),
-        load(3, dense_down, down_w),
+        load(4, dense_gate, gate_w.at[core]), load(5, dense_up, up_w.at[core]),
+        load(6, dense_down, down_w), load(7, mix_in, mix),
     ]
-    out_load.wait()
-    partial[...] = f32_dot(inner[...], out_w[...]).astype(BF16)
-    expert_loads = [
-        load(4, expert_gate, wide_gate), load(5, expert_up, wide_up),
-        load(6, expert_down, wide_down),
-    ]
+    first_loads[0].wait()
     greeted()
     swap = send(partial, other, swap_sem.at[0], swap_sem.at[1], place.sibling())
-    here = place.spot(0, 0, 0)
-    for d in range(1, ep_count):
-        target = (me + d) % ep_count
-        expert = target // (ep_count // EXPERTS)
-        send(
-            notes_in.at[expert], notes.at[here], note_send.at[d - 1], note_recv.at[d - 1],
-            everyone[d - 1],
-        )
-    notes[here] = notes_in[me // (ep_count // EXPERTS)]
+    expert_loads = [
+        load(8, expert_gate, wide_gate), load(9, expert_up, wide_up),
+        load(10, expert_down, wide_down),
+    ]
+    for copy in first_loads[1:]:
+        copy.wait()
     swap.wait_recv()
     middle = stream[...].astype(F32) + (partial[...].astype(F32) + other[...].astype(F32))
     hidden[...] = middle
@@ -381,6 +387,8 @@
 
     def pass_on(off, step):
         there = slot(*(o - s for o, s in zip(off, step)))
+        note = notes.at[place.spot(*off)]
+        send(note, note, note_send.at[used[0]], note_recv.at[there], place.near(*step))
         send(
             block(off), block(off), link_send.at[used[0]], link_recv.at[there], place.near(*step)
         )
@@ -388,6 +396,7 @@
 
     def arrived(off):
         at = slot(*off)
+        landed(notes.at[place.spot(*off)], note_recv.at[at])
         landed(block(off), link_recv.at[at])
         send(block(off), block(off), core_send.at[at], core_recv.at[at], place.sibling())
 
@@ -398,18 +407,29 @@
         send(
             src, dst.at[core], weight_sem.at[2 * i], weight_sem.at[2 * i + 1], place.sibling()
         )
-    for dz in zs:
-        if dz:
+    def straight(i):
+        return i >= line - STRAIGHT_OUT
+
+    def a_stage(i):
+        for da in range(1, side):
+            arrived((0, da, zs[i]))
+            for d in range(1, 1 if straight(i) else side):
+                pass_on((0, da, zs[i]), (d, 0, 0))
+
+    for i, dz in enumerate(zs):
+        if i:
             arrived((0, 0, dz))
         for d in range(1, side):
             pass_on((0, 0, dz), (0, d, 0))
         for d in range(1, side):
             pass_on((0, 0, dz), (d, 0, 0))
-    for dz in zs:
-        for da in range(1, side):
-            arrived((0, da, dz))
+        if straight(i):
             for d in range(1, side):
-                pass_on((0, da, dz), (d, 0, 0))
+                for da in range(1, side):
+                    pass_on((0, 0, dz), (d, da, 0))
+        if i:
+            a_stage(i - 1)
+    a_stage(line - 1)
 
     def planes_of(db):
         return [(db, da) for da in range(side)]
@@ -448,25 +468,41 @@
                 arrived((db, da, dz))
     for db in range(1, side):
         dense_in(planes_of(db))
-    for d in range(1, ep_count):
-        source = (me + ep_count - d) % ep_count
-        at = (source % (side * side)) * line + source // (side * side)
-        landed(notes.at[at], note_recv.at[d - 1])
+    lanes = notes.shape[2]
+    expert = (me // (ep_count // EXPERTS)).astype(F32)
+    named = [
+        (notes[:, TOP_K + k, :] == expert) & (iota((ep_count, lanes), 1) < row_count)
+        for k in range(TOP_K)
+    ]
+    hits = functools.reduce(jnp.logical_or, named)
+    before = iota((lanes, lanes), 0) < iota((lanes, lanes), 1)
+    rank = f32_dot(
+        jnp.where(hits, 1.0, 0.0).astype(BF16), jnp.where(before, 1.0, 0.0).astype(BF16)
+    )
+    rank = jnp.where(hits, rank + 1.0, 0.0).astype(BF16)
+    weight = sum(jnp.where(named[k], notes[:, k, :], 0.0) for k in range(TOP_K))
+    lay = iota((lanes, span), 0) == iota((lanes, span), 1) % row_count
+    lay = jnp.where(lay, 1.0, 0.0).astype(BF16)
+    chip = iota((ep_count, span), 0)
+    for k, parts in enumerate(([rank], parts_of(weight, 3))):
+        laid = sum(f32_dot(piece, lay) for piece in parts[::-1])
+        for at in range(side * side):
+            mine = chip == at * line + iota((ep_count, span), 1) // row_count
+            info[k, at] = jnp.sum(jnp.where(mine, laid, 0.0), axis=0, keepdims=True)
 
     def matches(at):
-        info = notes[group(at, line)].sum(axis=0)
         slot_id = iota((slots, span), 0)
         row_id = iota((slots, span), 1)
         hit = (slot_id // CAP == row_id // row_count) & (
-            (slot_id % CAP + 1).astype(F32) == info[0:1]
+            (slot_id % CAP + 1).astype(F32) == info[0, at]
         )
-        return hit, info[1:2]
+        return hit, info[1, at]
 
     planes = [(db, da) for db in range(side) for da in range(side)]
     for db, da in planes:
         at = place.plane(db, da)
-        for dz in zs:
-            if db or da or dz:
+        for i, dz in enumerate(zs):
+            if db or da or i:
                 theirs = every.at[place.spot(db, da, dz), other_rows(core, part)]
                 landed(theirs, core_recv.at[slot(da, db, dz)])
         hit, _ = matches(at)
@@ -498,6 +534,7 @@
         own[:, at : at + TILE] = results(core, at)
 
     dense_loads[2].wait()
+    dense_loads[3].wait()
     mixed = jax.nn.sigmoid(mix[...])
 
     def dense_out(db, da):
@@ -520,7 +557,7 @@
         back = f32_dot(pick, share[group(at, slots), :])
         dense[group(at, span), :] = dense[group(at, span), :] + back
 
-    order = place.z_order() + [0]
+    order = zs[::-1]
     used[0] = 0
 
     def block_of(off):
@@ -536,32 +573,55 @@
         landed(ref, sem)
         return value + ref[...].astype(F32)
 
-    for da in list(range(1, side)) + [0]:
+    das = list(range(1, side)) + [0]
+    for da in das:
         for db in range(1, side):
             result(db, da)
-            for dz in order:
+    for i, dz in enumerate(order):
+        for da in das:
+            for db in range(1, side):
+                value = block_of((db, da, dz))
+                if da and i < STRAIGHT_BACK:
+                    to = (db - 1, da - 1, dz)
+                    give_to(value, from_d.at[to], recv_d.at[to], (db, da, 0))
+                    continue
                 give_to(
-                    block_of((db, da, dz)), from_b.at[db - 1, da, dz], recv_b.at[db - 1, da, dz],
-                    (db, 0, 0),
+                    value, from_b.at[db - 1, da, dz], recv_b.at[db - 1, da, dz], (db, 0, 0)
                 )
-    for da in list(range(1, side)) + [0]:
+    for da in das:
         dense_out(0, da)
         result(0, da)
-        for dz in order:
-            value = block_of((0, da, dz))
-            for d in range(1, side):
-                value = add(value, from_b.at[d - 1, da, dz], recv_b.at[d - 1, da, dz])
-            if da:
-                give_to(value, from_a.at[da - 1, dz], recv_a.at[da - 1, dz], (0, da, 0))
-                continue
-            for d in range(1, side):
-                value = add(value, from_a.at[d - 1, dz], recv_a.at[d - 1, dz])
-            if dz:
-                give_to(value, from_z.at[dz - 1], recv_z.at[dz - 1], (0, 0, dz))
-                continue
-            for d in range(1, line):
-                value = add(value, from_z.at[d - 1], recv_z.at[d - 1])
-            out[...] = (hidden[:, my_half] + value).astype(out.dtype)
+
+    def after_b(da, i):
+        dz = order[i]
+        value = block_of((0, da, dz))
+        for d in range(1, 1 if da and i < STRAIGHT_BACK else side):
+            value = add(value, from_b.at[d - 1, da, dz], recv_b.at[d - 1, da, dz])
+        return value
+
+    def a_sums(i):
+        dz = order[i]
+        for da in range(1, side):
+            give_to(after_b(da, i), from_a.at[da - 1, dz], recv_a.at[da - 1, dz], (0, da, 0))
+
+    def after_a(i):
+        dz = order[i]
+        value = after_b(0, i)
+        for d in range(1, side):
+            value = add(value, from_a.at[d - 1, dz], recv_a.at[d - 1, dz])
+        if i < STRAIGHT_BACK:
+            for to in [(d, da, dz) for d in range(side - 1) for da in range(side - 1)]:
+                value = add(value, from_d.at[to], recv_d.at[to])
+        return value
+
+    a_sums(0)
+    for i, dz in enumerate(order[:-1]):
+        a_sums(i + 1)
+        give_to(after_a(i), from_z.at[dz - 1], recv_z.at[dz - 1], (0, 0, dz))
+    value = hidden[:, my_half] + after_a(line - 1)
+    for dz in zs[1:]:
+        value = add(value, from_z.at[line - dz - 1], recv_z.at[line - dz - 1])
+    out[...] = value.astype(out.dtype)
     for copy in sends:
         copy.wait_send()
 
@@ -571,7 +631,7 @@
 
 
 def ffn(
-    inner, stream, gain, notes, mix, mixer_out, dense_gate, dense_up, dense_down,
+    partial, stream, gain, note, mix, dense_gate, dense_up, dense_down,
     expert_gate, expert_up, expert_down,
 ):
     ep_count = lax.axis_size("ep")
@@ -596,14 +656,15 @@
     return pl.pallas_call(
         functools.partial(ffn_kernel, ep_count),
         out_shape=jax.ShapeDtypeStruct(block, BF16),
-        in_specs=[vmem] * 5 + [any_space] * 7,
+        in_specs=[any_space] * 11,
         out_specs=vmem,
         scratch_shapes=[
-            half_words(*mixer_out.shape),
+            half_words(row_count, width), words(1, width), words(1, half),
+            words(2, side * side, 1, line * row_count),
             half_words(2, units, half), half_words(2, units, half), half_words(units, half),
             half_words(width, deep), half_words(width, deep), half_words(deep, width),
             half_words(row_count, width), half_words(row_count, width), words(row_count, width),
-            half_words(ep_count, row_count, width), words((ep_count), *notes.shape[1:]),
+            half_words(ep_count, row_count, width), words(ep_count, *note.shape),
             half_words(ep_count, row_count, units),
             half_words(slots, width), half_words(slots, deep),
             words(ep_count * row_count, half),
@@ -611,18 +672,19 @@
             half_words(slots, half),
             half_words(ep_count, *block), half_words(more, side, line, *block),
             half_words(more, line, *block), half_words(max(line - 1, 1), *block),
-            dma((7,)), dma((2,)), dma((ep_count,)), dma((ep_count,)),
+            half_words(more, more, line, *block),
+            dma((11,)), dma((2,)), dma((ep_count,)), dma((ep_count,)),
             dma((ep_count,)), dma((ep_count,)), dma((ep_count,)), dma((ep_count,)),
             dma((4,)), dma((side * side,)), dma((side * side,)), dma((2,)),
             dma((ep_count,)), dma((more, side, line)), dma((more, line)),
-            dma((max(line - 1, 1),)),
+            dma((max(line - 1, 1),)), dma((more, more, line)),
         ],
         compiler_params=pltpu.CompilerParams(
             collective_id=1, has_side_effects=True, vmem_limit_bytes=60 * 1024 * 1024
         ),
         name="ffn",
     )(
-        inner, stream, gain, notes, mix, mixer_out, dense_gate, dense_up, dense_down,
+        partial, stream, gain, note, mix, dense_gate, dense_up, dense_down,
         expert_gate, expert_up, expert_down,
     )
 
@@ -633,13 +695,13 @@
     channel_gain, expert_ids, expert_weight, expert_gate, expert_up, expert_down,
     dense_gate, dense_up, dense_down, dense_mix,
 ):
-    inner, state_out, notes = mix_heads(
+    partial, state_out, note = mix_heads(
         stream, mixer_gain, gate_proj, input_proj, state_maps, step_proj, step_bias, decay_rate,
         input_taps, map_taps, input_past, map_past, head_state, skip_gain, inner_gain,
-        expert_ids, expert_weight,
+        expert_ids, expert_weight, mixer_out,
     )
     updated = ffn(
-        inner, stream, channel_gain[None, :], notes, dense_mix[None, :], mixer_out,
+        partial, stream, channel_gain[None, :], note, dense_mix[None, :],
         dense_gate.T, dense_up.T, dense_down, expert_gate, expert_up, expert_down,
     )
     return (updated, state_out)

time: 65.3 us -> 56.1 us (0.86)
  Pallas kernels: 62.9 us -> 53.8 us
    pallas_call x1, Pallas kernels: 14.2 us -> 8.61 us  [mix_heads(): pl.pallas_call(mix_kernel, out_shape=(jax.ShapeDtypeStruct((row_count, mi...]
    pallas_call x1, Pallas kernels: 48.7 us -> 45.2 us  [ffn(): pl.pallas_call(functools.partial(ffn_kernel, ep_count), out_shape=jax.Sha...]
where the time goes in v2:
time: 56.1 us; the launch traced here: 55.9 us
  Pallas kernels  53.8 us (96%)
  local copies, waits for them, and re-layouts  1.47 us (3%)
  between operations  0.65 us (1%)
    pallas_call x1, Pallas kernels, ffn(): pl.pallas_call(functools.partial(ffn_kernel, ep_count), out_shape=jax.Sha...  45.2 us
    pallas_call x1, Pallas kernels, mix_heads(): pl.pallas_call(mix_kernel, out_shape=(jax.ShapeDtypeStruct((row_count, mi...  8.61 us
    unnamed x1, local copies, waits for them, and re-layouts  1.47 us

profile of v2, /device:TPU:0, one launch (start us, length us, event | category | flops | bytes accessed | tf_op | source)
XLA Modules:
  0.0 55.9 jit_solution(2608673685471934130)
XLA Ops:
  0.6 8.6 %mix.1 = (bf16[32,2048]{1,0:T(8,128)(2,1)}, f32[256,4096]{1,0:T(8,128)}, f32[4,128]{1,0:T(4,128)}) custom-call(f32[8]{0:T(128)} %step_bias.1, f32[8]{0:T(128)} %decay_rate.1, f32[8]{0:T(128)} %skip_gain.1, bf16[32,2048]{1,0:T(8,128)(2,1)} %refs_1_.1, f32[1,2048]{1,0:T(1,128)} %bitcast.22, s32[2,32]{1,0:T(2,128)} %bitcast.25, f32[2,32]{1,0:T(2,128)} %bitcast.26, ...), custom_call_target="tpu_custom_call" | custom-call | tf_op jit(solution)/shard_map/mix/pallas_call | solution.py:237
  9.3 45.2 %ffn.1 = bf16[32,1024]{1,0:T(8,128)(2,1)} custom-call(bf16[32,2048]{1,0:T(8,128)(2,1)} %get-tuple-element.5.refs_0_, bf16[32,2048]{1,0:T(8,128)(2,1)} %refs_1_.1, f32[1,2048]{1,0:T(1,128)} %bitcast.21, f32[4,128]{1,0:T(4,128)} %get-tuple-element.6.refs_3_, f32[1,1024]{1,0:T(1,128)} %bitcast.23, bf16[352,1024]{1,0:T(8,128)(2,1)} %bitcast.16, ...), custom_call_target="tpu_custom_call" | custom-call | tf_op jit(solution)/shard_map/ffn/pallas_call | solution.py:656
  54.5 1.5 %copy.29 = bf16[32,1024]{1,0:T(8,128)(2,1)} copy(bf16[32,1024]{1,0:T(8,128)(2,1)} %ffn.1) | data formatting | bytes 131072
